TPU v7x, 256 devices: a whole 4x4x8 slice. The times are simulated.
256 devices in a mesh: ep: 16 (over y, x), tp: 16 (over z, core).
Axes of the slice: x: 4, y: 4, z: 8, core: 2. Of those that a mesh axis runs over, the one named last changes fastest.
Arguments:
- tokens: bfloat16 [4096, 4096], P('ep'), may hold values from -6 to 6
- cotangent: bfloat16 [4096, 4096], P('ep'), may hold values from -6 to 6
- routing: int32 [4096, 2], P('ep'), may hold values from 0 to 15, all different within a row; in each aligned block of 256 rows (0 to 255, 256 to 511, ...) at most 40 rows name the same one
- group_gate: float32 [4096], P('ep'), may hold values from 0.2 to 1
- inner_gate: float32 [4096, 2], P('ep'), may hold values from 0.1 to 0.9
- w_gate: bfloat16 [16, 4096, 2048], P('ep', None, 'tp'), may hold values from -0.09375 to 0.09375
- w_up: bfloat16 [16, 4096, 2048], P('ep', None, 'tp'), may hold values from -0.09375 to 0.09375
- w_down: bfloat16 [16, 2048, 4096], P('ep', 'tp'), may hold values from -0.125 to 0.125
Outputs:
- token_grad: bfloat16 [4096, 4096], P('ep', 'tp')
- group_grad: float32 [4096], P('ep')
- inner_grad: float32 [4096, 2], P('ep')
- gate_weight_grad: bfloat16 [16, 4096, 2048], P('ep', None, 'tp')
- up_weight_grad: bfloat16 [16, 4096, 2048], P('ep', None, 'tp')
- down_weight_grad: bfloat16 [16, 2048, 4096], P('ep', 'tp')
Inputs may be any that keep to these rules, and one draw needn't show every extreme that they name: `routing`: each row names 2 different experts. Among the rows of one device (aligned blocks of 256 rows) no expert is named more than 40 times, and in every draw some expert is named exactly 40 times in some block.
All inputs are finite; a program needn't handle non-finite values.
Results may differ from a plain program's by a relative error of at most 0.02.
Values may be sent and summed in bfloat16 or wider, within the bound.
No kernel may reach another device: no remote copies, remote signals or barrier semaphores. Data moves between devices by JAX's collectives and lax.ppermute only.
A program may use at most 128 MiB of HBM per device.

v0:
```python
import jax
import jax.numpy as jnp
from jax import lax
from jax.experimental import pallas as pl
from jax.experimental.pallas import tpu as pltpu
from jax.sharding import Mesh, PartitionSpec as P


BF = jnp.bfloat16
F32 = jnp.float32
I32 = jnp.int32
UNIT = 512
WIRE = 640
A_UNITS = 5
B_UNITS = 3
WHOLE = pl.BlockSpec(memory_space=pltpu.VMEM)
FAR = pl.BlockSpec(memory_space=pltpu.HBM)
SCALARS = pl.BlockSpec(memory_space=pltpu.SMEM)


def iota(shape, dim):
    return lax.broadcasted_iota(I32, shape, dim)


def as_bf(mask):
    return jnp.where(mask, 1.0, 0.0).astype(BF)


def mm(a, b, ca=1, cb=0):
    return lax.dot_general(a, b, (((ca,), (cb,)), ((), ())), preferred_element_type=F32)


def fold_matrix():
    o = iota((256, 256), 0)
    i = iota((256, 256), 1)
    return as_bf(((o >> 6) == ((i >> 2) & 3)) & (((o >> 2) & 15) == (i >> 4)) & ((o & 3) == (i & 3)))


def expert_rows():
    return as_bf((iota((256, 128), 0) >> 4) == iota((256, 128), 1))


def pack_unit(ohm, oht, src, out):
    row = iota((256, 256), 0)
    out[:, :UNIT] = mm(ohm, src[...]).astype(BF)
    tail = jnp.zeros((256, 128), F32)
    for q in range(4):
        tail += mm(jnp.where(((row >> 2) & 3) == q, oht, jnp.zeros_like(oht)), src[:, q * 128 : q * 128 + 128])
    out[:, UNIT:WIRE] = tail.astype(BF)


def pack_a(s_ref, r_ref, x_ref, g_ref, a_ref, info_ref, ohm_ref, oht_ref, src, dst, sem_in, sem_out):
    def fetch(ref, u):
        return pltpu.make_async_copy(ref.at[:, u * UNIT : (u + 1) * UNIT], src.at[u], sem_in.at[u])

    for u in range(A_UNITS):

        @pl.when(s_ref[0] == 0)
        def _(u=u):
            fetch(x_ref, u).start()

        @pl.when(s_ref[0] != 0)
        def _(u=u):
            fetch(g_ref, u).start()

    r = r_ref[...]
    expert = iota((128, 256), 0)
    named = (r[0:1, :] == expert) | (r[1:2, :] == expert)
    ti = iota((256, 256), 0)
    tj = iota((256, 256), 1)
    rank = mm(as_bf(named), as_bf(ti < tj))
    for k in range(2):
        info_ref[2 * k : 2 * k + 1, :] = r[k : k + 1, :].astype(F32)
        mine = jnp.where(r[k : k + 1, :] == expert, rank, 0.0)
        info_ref[2 * k + 1 : 2 * k + 2, :] = jnp.sum(mine, axis=0, keepdims=True)
    info_ref[4:8, :] = jnp.zeros((4, 256), F32)
    spread = mm(expert_rows(), jnp.where(named, rank, -1.0).astype(BF)).astype(I32)
    first = s_ref[1] * 20
    ohm_ref[...] = as_bf(spread == first + (ti & 15))
    oht_ref[...] = as_bf(spread == first + 16 + (ti & 3))

    outs = []
    for u in range(A_UNITS):
        fetch(x_ref, u).wait()
        pack_unit(ohm_ref[...], oht_ref[...], src.at[u], dst.at[u])
        out = pltpu.make_async_copy(dst.at[u], a_ref.at[:, u * WIRE : (u + 1) * WIRE], sem_out.at[u])
        out.start()
        outs.append(out)
    for out in outs:
        out.wait()


def pack_b(r_ref, gg_ref, ig_ref, info_ref, ohm_ref, oht_ref, x_ref, g_ref, bx_ref, bg_ref, wt_ref, mask_ref):
    ohm = ohm_ref[...]
    oht = oht_ref[...]
    pack_unit(ohm, oht, x_ref, bx_ref)
    pack_unit(ohm, oht, g_ref, bg_ref)

    @pl.when(pl.program_id(0) == 0)
    def _():
        r = r_ref[...]
        expert = iota((128, 256), 0)
        comb = gg_ref[...] * ig_ref[...]
        w = jnp.where(r[0:1, :] == expert, comb[0:1, :], 0.0) + jnp.where(r[1:2, :] == expert, comb[1:2, :], 0.0)
        hi = w.astype(BF)
        lo = (w - hi.astype(F32)).astype(BF)

        def picked(oh, part):
            return jnp.sum(oh.astype(F32) * mm(expert_rows(), part), axis=1, keepdims=True)

        lane = iota((256, 128), 1)
        vals = jnp.where(lane == 0, picked(ohm, hi), 0.0)
        vals = jnp.where(lane == 1, picked(ohm, lo), vals)
        vals = jnp.where(lane == 2, picked(oht, hi), vals)
        vals = jnp.where(lane == 3, picked(oht, lo), vals)
        wt_ref[...] = vals.astype(BF)

        eye = as_bf(iota((256, 256), 0) == iota((256, 256), 1))
        cols = mm(eye, info_ref[...].astype(BF), 1, 1).astype(I32)
        slot = iota((256, 512), 1)
        for k in range(2):
            here = (slot >> 5) == cols[:, 2 * k : 2 * k + 1]
            left = cols[:, 2 * k + 1 : 2 * k + 2] - 20 * ((slot >> 4) & 1)
            mask_ref[k, :, :] = as_bf(here & (left == (slot & 15)))
            mask_ref[2 + k, :, :] = as_bf(here & (left == 16 + (slot & 3)))


def wire(u):
    return slice(u * WIRE, (u + 1) * WIRE)


def cols(u):
    return slice(u * UNIT, (u + 1) * UNIT)


def unpack(fold, buf, dst, u):
    dst[0:256, cols(u)] = buf[:, 0:UNIT]
    t = mm(fold, buf[:, UNIT:WIRE]).astype(BF)
    for q in range(4):
        dst[256:320, u * UNIT + q * 128 : u * UNIT + q * 128 + 128] = t[q * 64 : q * 64 + 64, :]


def expert_kernel(s_ref, a_ref, z1_ref, z2_ref, b_ref, wcat_ref, wd_hbm,
                  x_hbm, g_hbm, c_hbm, hid_hbm, in_hbm, sc_hbm, up_hbm, dn_hbm,
                  buf_a, buf_z, buf_b, wt_buf, wc, wd, xv, gv, pre_acc, gh_acc,
                  c_out, hid_out, in_out, sc_out, up_out, dn_out, sem_i, sem_w, sem_o):
    units = A_UNITS + B_UNITS
    at = 2 * B_UNITS * WIRE
    in_wt = pltpu.make_async_copy(b_ref.at[:, at : at + 128], wt_buf, sem_w.at[2 * units])
    loads = []
    for u in range(units):
        if u < A_UNITS:
            rows = [
                pltpu.make_async_copy(a_ref.at[:, wire(u)], buf_a.at[u], sem_i.at[3 * u]),
                pltpu.make_async_copy(z1_ref.at[:, wire(u)], buf_z.at[u, 0:128], sem_i.at[3 * u + 1]),
                pltpu.make_async_copy(z2_ref.at[:, wire(u)], buf_z.at[u, 128:256], sem_i.at[3 * u + 2]),
            ]
        else:
            n = u - A_UNITS
            m = n + B_UNITS
            rows = [
                pltpu.make_async_copy(b_ref.at[:, wire(n)], buf_b.at[n], sem_i.at[3 * u]),
                pltpu.make_async_copy(b_ref.at[:, wire(m)], buf_b.at[m], sem_i.at[3 * u + 1]),
            ]
        weights = [
            pltpu.make_async_copy(wcat_ref.at[cols(u)], wc.at[cols(u)], sem_w.at[2 * u]),
            pltpu.make_async_copy(wd_hbm.at[:, cols(u)], wd.at[:, cols(u)], sem_w.at[2 * u + 1]),
        ]
        for copy in rows + weights:
            copy.start()
        loads.append((rows, weights))
    in_wt.start()
    outs = []

    def send(src, dst):
        outs.append(pltpu.make_async_copy(src, dst, sem_o.at[len(outs)]))
        outs[-1].start()

    fold = fold_matrix()
    fold0 = fold[0:64, :]
    lane = iota((256, 128), 1)
    for u in range(units):
        for copy in loads[u][0]:
            copy.wait()
        if u < A_UNITS:

            @pl.when(s_ref[0] == 0)
            def _(u=u):
                unpack(fold, buf_a.at[u], xv, u)
                unpack(fold, buf_z.at[u], gv, u)

            @pl.when(s_ref[0] != 0)
            def _(u=u):
                unpack(fold, buf_a.at[u], gv, u)
                unpack(fold, buf_z.at[u], xv, u)
        else:
            unpack(fold, buf_b.at[u - A_UNITS], xv, u)
            unpack(fold, buf_b.at[u - A_UNITS + B_UNITS], gv, u)
        for copy in loads[u][1]:
            copy.wait()
        if u % 2 == 1:
            both = slice((u - 1) * UNIT, (u + 1) * UNIT)
            send(xv.at[:, both], x_hbm.at[:, both])
            send(gv.at[:, both], g_hbm.at[:, both])
            p = mm(xv[:, both], wc[both, :])
            g = mm(gv[:, both], wd[:, both], 1, 1)
            if u > 1:
                p += pre_acc[...]
                g += gh_acc[...]
            pre_acc[...] = p
            gh_acc[...] = g
    in_wt.wait()
    wt = wt_buf[...]
    wt_f = wt.astype(F32)
    c_main = wt_f[:, 0:1] + wt_f[:, 1:2]
    wt_t = mm(fold0, wt)
    c_tail = wt_t[:, 2:3] + wt_t[:, 3:4]

    def activations(at, count, c):
        gate_pre = pre_acc[at : at + count, 0:256]
        up_pre = pre_acc[at : at + count, 256:512]
        g = gh_acc[at : at + count, :]
        sig = jax.nn.sigmoid(gate_pre)
        silu = gate_pre * sig
        hid = (silu * up_pre).astype(BF)
        score = jnp.sum(g * hid.astype(F32), axis=1, keepdims=True)
        weighted = c * g
        in_out[at : at + count, 0:256] = (weighted * up_pre * sig * (1.0 + gate_pre * (1.0 - sig))).astype(BF)
        in_out[at : at + count, 256:512] = (weighted * silu).astype(BF)
        hid_out[at : at + count, :] = hid
        c_out[at : at + count, :] = jnp.broadcast_to(c, (count, 128))
        hi = score.astype(BF).astype(F32)
        return hi, score - hi

    hi_m, lo_m = activations(0, 256, c_main)
    hi_t, lo_t = activations(256, 64, c_tail)
    lane_t = iota((64, 128), 1)
    tails = jnp.where(lane_t == 2, hi_t, jnp.where(lane_t == 3, lo_t, 0.0)).astype(BF)
    vals = jnp.where(lane == 0, hi_m, jnp.where(lane == 1, lo_m, 0.0)) + mm(fold0, tails, 0, 0)
    vals = vals.astype(BF)
    sc_out[...] = vals
    dn_out[0:256, 1024:1152] = vals
    dn_out[256:320, 1024:1152] = jnp.zeros((64, 128), BF)
    send(in_out, in_hbm)
    send(hid_out, hid_hbm)
    send(c_out, c_hbm)
    send(sc_out, sc_hbm)

    ins = in_out[...]
    for i in range(4):
        dst = up_out if i < 2 else dn_out
        for c in range(2):
            at = pl.multiple_of((2 * i + 1 - s_ref[0]) * 512 + c * 256, 256)
            col = (i % 2) * 512 + c * 256
            dst[:, col : col + 256] = mm(ins, wc[pl.ds(at, 256), :], 1, 1).astype(BF)
        if i == 1:
            send(up_out, up_hbm)
    send(dn_out, dn_hbm)
    for copy in outs:
        copy.wait()


def return_kernel(s_ref, in_ref, wcat_ref, sc_ref, up_ref, dn_ref, out_ref):
    fold = fold_matrix()
    ins = in_ref[...]
    lane = iota((256, 128), 1)
    s = sc_ref[...].astype(F32) + dn_ref[0:256, 1024:1152].astype(F32)
    s = s + pltpu.roll(s, 127, 1)
    hi = s.astype(BF).astype(F32)
    vals = jnp.where((lane & 1) == 0, hi, pltpu.roll(s - hi, 1, 1)).astype(BF)
    for c in range(2):
        for u in range(2):
            src = (up_ref, dn_ref)[u]
            tails = []
            for h in range(2):
                at = pl.multiple_of((4 * u + 2 * h + s_ref[0]) * 512 + c * 256, 256)
                col = h * 512 + c * 256
                part = mm(ins, wcat_ref[pl.ds(at, 256), :], 1, 1) + src[0:320, col : col + 256].astype(F32)
                part = part.astype(BF)
                for b in range(16):
                    out_ref[2 * b + c, :, u * WIRE + h * 256 : u * WIRE + h * 256 + 256] = part[16 * b : 16 * b + 16, :]
                tails += [part[256:320, 0:128], part[256:320, 128:256]]
            folded = mm(fold, jnp.concatenate(tails, axis=0), 0, 0).astype(BF)
            for b in range(16):
                out_ref[2 * b + c, :, u * WIRE + UNIT : (u + 1) * WIRE] = folded[16 * b : 16 * b + 16, :]
        for b in range(16):
            out_ref[2 * b + c, :, 2 * WIRE :] = vals[16 * b : 16 * b + 16, :]


def combine_kernel(s_ref, mask_ref, r1_ref, *outs):
    acc_ref = outs[4]
    slot = iota((256, 512), 1)
    zero = jnp.zeros((256, 512), BF)
    main = mask_ref[0] + mask_ref[1]
    tail_any = mask_ref[2] + mask_ref[3]
    tails = [jnp.where(((slot >> 2) & 3) == q, tail_any, zero) for q in range(4)]
    for u in range(2):
        full = mm(main, r1_ref[:, u * WIRE : u * WIRE + UNIT])
        tail = r1_ref[:, u * WIRE + UNIT : (u + 1) * WIRE]
        for q in range(4):
            acc_ref[:, u * UNIT + q * 128 : u * UNIT + q * 128 + 128] = (
                full[:, q * 128 : q * 128 + 128] + mm(tails[q], tail)
            ).astype(BF)
    sc = r1_ref[:, 2 * WIRE :]
    rows = []
    for k in range(2):
        m = mm(sc, mask_ref[k], 0, 1)
        t = mm(sc, jnp.where(((slot >> 2) & 3) == 0, mask_ref[2 + k], zero), 0, 1)
        score = m[0:1, :] + m[1:2, :] + t[2:3, :] + t[3:4, :]
        hi = score.astype(BF).astype(F32)
        rows += [hi, score - hi]
    row16 = iota((16, 256), 0)
    scores = jnp.zeros((16, 256), F32)
    for n in range(4):
        scores = jnp.where(row16 == n, rows[n], scores)
    scores = scores.astype(BF)
    for n in range(4):
        dest = lax.rem(s_ref[2] + 2 * n, 8)
        at = pl.multiple_of((dest >> 1) * 256, 256)
        outs[n][0:256, :] = acc_ref[:, pl.ds(at, 256)]
        outs[n][256:272, :] = scores


def final_kernel(gg_ref, ig_ref, p0, p1, p2, p3, tok_ref, group_ref, inner_ref):
    total = p0[...].astype(F32) + p1[...].astype(F32) + p2[...].astype(F32) + p3[...].astype(F32)
    tok_ref[...] = total[0:256, :].astype(BF)
    s0 = total[256:257, :] + total[257:258, :]
    s1 = total[258:259, :] + total[259:260, :]
    gg = gg_ref[...]
    inner_ref[0:1, :] = gg * s0
    inner_ref[1:2, :] = gg * s1
    group_ref[...] = ig_ref[0:1, :] * s0 + ig_ref[1:2, :] * s1


def sds(shape, dtype=BF):
    return jax.ShapeDtypeStruct(shape, dtype)


def call(kernel, outs, ins, mib, scalars=True, out_specs=None, **kw):
    specs = ([SCALARS] if scalars else []) + list(ins)
    return pl.pallas_call(
        kernel,
        out_shape=outs,
        in_specs=specs,
        out_specs=out_specs or jax.tree.map(lambda _: WHOLE, outs),
        compiler_params=pltpu.CompilerParams(vmem_limit_bytes=mib * 2**20),
        **kw,
    )


def vmem(*shape):
    return pltpu.VMEM(shape, BF)


def sems(n):
    return pltpu.SemaphoreType.DMA((n,))


def around(k):
    return [(i, (i + k) % 8) for i in range(8)]


def tdot(a, b):
    return lax.dot_general(a, b, (((0,), (0,)), ((), ())), preferred_element_type=F32)


def per_device(tokens, cotangent, routing, group_gate, inner_gate, w_gate, w_up, w_down):
    z = lax.axis_index("z")
    info = jnp.stack([z % 2, lax.axis_index("core"), z]).astype(I32)
    gg = group_gate[None, :]
    ig = inner_gate.T
    rt = routing.T

    swap = [(0, 1), (1, 0)]
    other = [lax.ppermute(w[0], "core", swap) for w in (w_gate, w_up, w_down)]

    whole = lambda i: (0, 0)
    block = lambda i: (0, i)
    later = lambda i: (0, A_UNITS + i)
    small = pltpu.CompilerParams(vmem_limit_bytes=12 * 2**20)
    a_send, ranks, ohm, oht = call(
        pack_a,
        (sds((256, A_UNITS * WIRE)), sds((8, 256), F32), sds((256, 256)), sds((256, 256))),
        (WHOLE, FAR, FAR),
        63,
        out_specs=(FAR, WHOLE, WHOLE, WHOLE),
        scratch_shapes=[
            vmem(A_UNITS, 256, UNIT), vmem(A_UNITS, 256, WIRE), sems(A_UNITS), sems(A_UNITS),
        ],
    )(info, rt, tokens, cotangent)
    a_recv = lax.all_to_all(a_send.reshape(16, 16, -1), "ep", 0, 0, tiled=True).reshape(256, -1)

    bx, bg, wt, masks = pl.pallas_call(
        pack_b,
        grid=(B_UNITS,),
        in_specs=[
            pl.BlockSpec((2, 256), whole),
            pl.BlockSpec((1, 256), whole),
            pl.BlockSpec((2, 256), whole),
            pl.BlockSpec((8, 256), whole),
            pl.BlockSpec((256, 256), whole),
            pl.BlockSpec((256, 256), whole),
            pl.BlockSpec((256, UNIT), later),
            pl.BlockSpec((256, UNIT), later),
        ],
        out_specs=(
            pl.BlockSpec((256, WIRE), block),
            pl.BlockSpec((256, WIRE), block),
            pl.BlockSpec((256, 128), whole),
            pl.BlockSpec((4, 256, 512), lambda i: (0, 0, 0)),
        ),
        out_shape=(
            sds((256, B_UNITS * WIRE)), sds((256, B_UNITS * WIRE)), sds((256, 128)), sds((4, 256, 512)),
        ),
        compiler_params=small,
    )(rt, gg, ig, ranks, ohm, oht, tokens, cotangent)
    b_send = jnp.concatenate([bx, bg, wt], axis=1)
    b_send, a_recv = lax.optimization_barrier((b_send, a_recv))
    z1 = lax.ppermute(a_recv[:128], "z", around(1))
    z2 = lax.ppermute(a_recv[128:], "z", around(-1))
    b_recv = lax.all_to_all(b_send.reshape(16, 16, -1), "ep", 0, 0, tiled=True).reshape(256, -1)
    wcat = jnp.concatenate([w_gate[0], other[0], w_up[0], other[1]], axis=1)
    wd = jnp.concatenate([w_down[0], other[2]], axis=0)

    outs = (
        sds((320, 4096)), sds((320, 4096)), sds((320, 128), F32), sds((320, 256)),
        sds((320, 512)), sds((256, 128)), sds((320, 1024)), sds((320, 1152)),
    )
    n = A_UNITS + B_UNITS
    xs, gs, cw, hid, ins, sc, up, dn = call(
        expert_kernel,
        outs,
        (FAR,) * 6,
        63,
        out_specs=(FAR,) * 8,
        scratch_shapes=[
            vmem(A_UNITS, 256, WIRE), vmem(A_UNITS, 256, WIRE), vmem(2 * B_UNITS, 256, WIRE), vmem(256, 128),
            vmem(4096, 512), vmem(256, 4096), vmem(320, 4096), vmem(320, 4096),
            pltpu.VMEM((320, 512), F32), pltpu.VMEM((320, 256), F32),
            pltpu.VMEM((320, 128), F32), vmem(320, 256), vmem(320, 512), vmem(256, 128),
            vmem(320, 1024), vmem(320, 1152), sems(3 * n), sems(2 * n + 1), sems(n + 6),
        ],
    )(info, a_recv, z1, z2, b_recv, wcat, wd)
    up = lax.ppermute(up, "z", around(1))
    dn = lax.ppermute(dn, "z", around(-1))

    scaled = (cw[:, 0:1] * gs).astype(BF)
    d_par = tdot(hid[:, 128:], scaled).astype(BF)
    g_par = tdot(xs, ins[:, 128:256]).astype(BF)
    u_par = tdot(xs, ins[:, 384:512]).astype(BF)
    d_par, g_par, u_par = [lax.ppermute(t, "core", swap) for t in (d_par, g_par, u_par)]

    p1 = call(return_kernel, sds((32, 16, 2 * WIRE + 128)), (WHOLE,) * 5, 8)(info, ins, wcat, sc, up, dn)
    r1 = lax.all_to_all(p1, ("ep", "core"), 0, 0, tiled=True).reshape(512, -1)

    down_grad = (tdot(hid[:, :128], scaled) + d_par).astype(BF)
    gate_grad = (tdot(xs, ins[:, 0:128]) + g_par).astype(BF)
    upper_grad = (tdot(xs, ins[:, 256:384]) + u_par).astype(BF)

    pieces = call(
        combine_kernel, (sds((272, 256)),) * 4, (WHOLE,) * 2, 8, scratch_shapes=[pltpu.VMEM((256, 1024), BF)]
    )(info, masks, r1)
    got = [lax.ppermute(pieces[n], "z", around(2 * n)) for n in (2, 1, 3)]
    token_grad, group_grad, inner_grad = call(
        final_kernel, (sds((256, 256)), sds((1, 256), F32), sds((2, 256), F32)), (WHOLE,) * 6, 4, scalars=False
    )(gg, ig, pieces[0], *got)
    return token_grad, group_grad[0], inner_grad.T, gate_grad[None], upper_grad[None], down_grad[None]


def solution(mesh):
    split = Mesh(mesh.devices.reshape(16, 8, 2), ("ep", "z", "core"))
    tp = ("z", "core")
    return jax.shard_map(
        per_device,
        mesh=split,
        in_specs=(
            P("ep", None), P("ep", None), P("ep", None), P("ep"), P("ep", None),
            P("ep", None, tp), P("ep", None, tp), P("ep", tp, None),
        ),
        out_specs=(
            P("ep", tp), P("ep"), P("ep", None), P("ep", None, tp), P("ep", None, tp), P("ep", tp, None),
        ),
        check_vma=False,
    )
```

profile of v0, /device:TPU:2, one launch (start us, length us, event | category | flops | bytes accessed | tf_op | source)
XLA Modules:
  0.0 153.0 jit_solution(4044713900561873321)
XLA Ops:
  1.3 5.0 %shard_map.127 = (bf16[256,3200]{1,0:T(8,128)(2,1)}, f32[8,256]{1,0:T(8,128)}, bf16[256,256]{1,0:T(8,128)(2,1)}, bf16[256,256]{1,0:T(8,128)(2,1)}) custom-call(s32[3]{0:T(128)} %pad_add_fusion.s_ref, s32[2,256]{1,0:T(2,128)} %bitcast.27, bf16[256,4096]{1,0:T(8,128)(2,1)} %x_ref.3, bf16[256,4096]{1,0:T(8,128)(2,1)} %g_ref.3), custom_call_target="tpu_custom_call" | custom-call | tf_op jit(solution)/shard_map/pallas_call | solution.py:381
  6.4 7.6 %all-to-all-start = ((bf16[16,16,3200]{2,1,0:T(8,128)(2,1)}), bf16[16,16,3200]{2,1,0:T(8,128)(2,1)}, u32[]{:S(2)}, u32[]{:S(2)}) async-start(bf16[16,16,3200]{2,1,0:T(8,128)(2,1)} %bitcast.33), calls=%async_computation | async-start | bytes 3276800 | tf_op jit(solution)/shard_map/all_to_all | solution.py:391
  16.3 3.2 %shard_map.128 = (bf16[256,1920]{1,0:T(8,128)(2,1)S(1)}, bf16[256,1920]{1,0:T(8,128)(2,1)S(1)}, bf16[256,128]{1,0:T(8,128)(2,1)S(1)}, bf16[4,256,512]{2,1,0:T(8,128)(2,1)S(1)}) custom-call(s32[2,256]{1,0:T(2,128)S(1)} %bitcast.28, f32[1,256]{1,0:T(1,128)S(1)} %bitcast.31, f32[2,256]{1,0:T(2,128)S(1)} %bitcast.29, f32[8,256]{1,0:T(8,128)S(1)} %copy-done.10, ...), custom_call_target="tpu_custom_call" | custom-call | tf_op jit(solution)/shard_map/pallas_call | solution.py:393
  21.9 14.4 %all-to-all-done = bf16[16,16,3200]{2,1,0:T(8,128)(2,1)} async-done(((bf16[16,16,3200]{2,1,0:T(8,128)(2,1)}), bf16[16,16,3200]{2,1,0:T(8,128)(2,1)}, u32[]{:S(2)}, u32[]{:S(2)}) %all-to-all-start) | async-done | bytes 1638432 | tf_op jit(solution)/shard_map/all_to_all | solution.py:391
  36.3 7.4 %all-to-all-start.1 = ((bf16[16,16,3968]{2,1,0:T(8,128)(2,1)}), bf16[16,16,3968]{2,1,0:T(8,128)(2,1)}, u32[]{:S(2)}, u32[]{:S(2)}) async-start(bf16[16,16,3968]{2,1,0:T(8,128)(2,1)} %bitcast.8), calls=%async_computation.1 | async-start | bytes 4063232 | tf_op jit(solution)/shard_map/all_to_all | solution.py:421
  45.4 5.9 %collective-permute-start.1 = (bf16[128,3200]{1,0:T(8,128)(2,1)S(1)}, bf16[128,3200]{1,0:T(8,128)(2,1)}, u32[]{:S(2)}, u32[]{:S(2)}) collective-permute-start(bf16[128,3200]{1,0:T(8,128)(2,1)S(1)} %get-tuple-element.56), channel_id=1, source_target_pairs={{0,14},{2,0},{4,2},{6,4},{8,6},{10,8},{12,10},{14,12},{1,15},{3,1}... | collective-permute-start | bytes 2457608 | tf_op jit(solution)/shard_map/ppermute | solution.py:420
  52.8 3.4 %pad_maximum_fusion.wcat_ref = bf16[4096,512]{1,0:T(8,128)(2,1)} fusion(bf16[4096,128]{1,0:T(8,128)(2,1)} %collective-permute-done.3, bf16[4096,128]{1,0:T(8,128)(2,1)S(1)} %bitcast.37, bf16[4096,128]{1,0:T(8,128)(2,1)} %collective-permute-done.2, bf16[4096,128]{1,0:T(8,128)(2,1)S(1)} %bitcast.39), kind=kLoop, calls=%fused_computation.13 | loop fusion | flops 16777216 | bytes 8388608 | tf_op jit(solution)/shard_map/concatenate | solution.py:422
  56.3 10.8 %collective-permute-done.1.z2_ref = bf16[128,3200]{1,0:T(8,128)(2,1)} collective-permute-done((bf16[128,3200]{1,0:T(8,128)(2,1)S(1)}, bf16[128,3200]{1,0:T(8,128)(2,1)}, u32[]{:S(2)}, u32[]{:S(2)}) %collective-permute-start.1) | collective-permute-done | bytes 819232 | tf_op jit(solution)/shard_map/ppermute | solution.py:420
  67.1 3.5 %collective-permute-done.z1_ref = bf16[128,3200]{1,0:T(8,128)(2,1)} collective-permute-done((bf16[128,3200]{1,0:T(8,128)(2,1)S(1)}, bf16[128,3200]{1,0:T(8,128)(2,1)}, u32[]{:S(2)}, u32[]{:S(2)}) %collective-permute-start) | collective-permute-done | bytes 819232 | tf_op jit(solution)/shard_map/ppermute | solution.py:419
  70.6 10.1 %shard_map.129 = (bf16[320,4096]{1,0:T(8,128)(2,1)}, bf16[320,4096]{1,0:T(8,128)(2,1)}, f32[320,128]{1,0:T(8,128)}, bf16[320,256]{1,0:T(8,128)(2,1)}, bf16[320,5...) custom-call(s32[3]{0:T(128)} %pad_add_fusion.s_ref, ...), custom_call_target="tpu_custom_call" | custom-call | tf_op jit(solution)/shard_map/pallas_call | solution.py:430
  80.7 4.4 %collective-permute-start.6 = (bf16[320,1152]{1,0:T(8,128)(2,1)}, bf16[320,1152]{1,0:T(8,128)(2,1)S(1)}, u32[]{:S(2)}, u32[]{:S(2)}) collective-permute-start(bf16[320,1152]{1,0:T(8,128)(2,1)} %get-tuple-element.44), channel_id=1, source_target_pairs={{0,14},{2,0},{4,2},{6,4},{8,6},{10,8},{12,10},{14,12},{1,15},{3,1}... | collective-permute-start | bytes 2211848 | tf_op jit(solution)/shard_map/ppermute | solution.py:445
  85.2 3.9 %convolution_convert_fusion.2 = bf16[4096,128]{1,0:T(8,128)(2,1)} fusion(bf16[320,4096]{1,0:T(8,128)(2,1)} %get-tuple-element.52, bf16[320,512]{1,0:T(8,128)(2,1)} %get-tuple-element.41.in_ref), kind=kOutput, calls=%fused_computation.9 | convolution fusion | flops 336068608 | bytes 3751936 | tf_op jit(solution)/shard_map/dot_general | solution.py:364
  91.2 10.2 %collective-permute-done.5.up_ref = bf16[320,1024]{1,0:T(8,128)(2,1)S(1)} collective-permute-done((bf16[320,1024]{1,0:T(8,128)(2,1)}, bf16[320,1024]{1,0:T(8,128)(2,1)S(1)}, u32[]{:S(2)}, u32[]{:S(2)}) %collective-permute-start.5) | collective-permute-done | bytes 655392 | tf_op jit(solution)/shard_map/ppermute | solution.py:444
  101.4 3.4 %shard_map.130 = bf16[32,16,1408]{2,1,0:T(8,128)(2,1)} custom-call(s32[3]{0:T(128)S(1)} %copy-done.9, bf16[320,512]{1,0:T(8,128)(2,1)S(1)} %copy-done.3, bf16[4096,512]{1,0:T(8,128)(2,1)S(1)} %copy-done, bf16[256,128]{1,0:T(8,128)(2,1)S(1)} %copy-done.8, bf16[320,1024]{1,0:T(8,128)(2,1)S(1)} %collective-permute-done.5.up_ref, ...), custom_call_target="tpu_custom_call" | custom-call | tf_op jit(solution)/shard_map/pallas_call | solution.py:453
  104.8 8.1 %all-to-all-start.2 = ((bf16[32,16,1408]{2,1,0:T(8,128)(2,1)}), bf16[32,16,1408]{2,1,0:T(8,128)(2,1)S(1)}, u32[]{:S(2)}, u32[]{:S(2)}) async-start(bf16[32,16,1408]{2,1,0:T(8,128)(2,1)} %shard_map.130), calls=%async_computation.2 | async-start | bytes 2883584 | tf_op jit(solution)/shard_map/all_to_all | solution.py:454
  113.2 3.8 %convolution_convert_fusion = bf16[128,4096]{1,0:T(8,128)(2,1)} fusion(bf16[320,4096]{1,0:T(8,128)(2,1)} %get-tuple-element.55, f32[320]{0:T(512)S(1)} %slice_reduce_fusion, bf16[320,256]{1,0:T(8,128)(2,1)S(1)} %copy-done.20), kind=kOutput, calls=%fused_computation.7 | convolution fusion | flops 340000768 | bytes 3753984 | tf_op jit(solution)/shard_map/dot_general | solution.py:364
  117.4 2.0 %fusion.5 = bf16[1,4096,128]{2,1,0:T(8,128)(2,1)} fusion(bf16[320,4096]{1,0:T(8,128)(2,1)S(1)} %copy-done.15, bf16[4096,128]{1,0:T(8,128)(2,1)S(1)} %collective-permute-done.10, bf16[320,512]{1,0:T(8,128)(2,1)S(1)} %copy-done.3), kind=kOutput, calls=%fused_computation.12 | convolution fusion | flops 337117184 | bytes 4800512 | tf_op jit(solution)/shard_map/dot_general | solution.py:364
  119.4 2.1 %fusion.4 = bf16[1,4096,128]{2,1,0:T(8,128)(2,1)} fusion(bf16[320,4096]{1,0:T(8,128)(2,1)S(1)} %copy-done.15, bf16[4096,128]{1,0:T(8,128)(2,1)S(1)} %collective-permute-done.11, bf16[320,512]{1,0:T(8,128)(2,1)S(1)} %copy-done.3), kind=kOutput, calls=%fused_computation.11 | convolution fusion | flops 337117184 | bytes 4800512 | tf_op jit(solution)/shard_map/dot_general | solution.py:364
  121.5 11.7 %all-to-all-done.2 = bf16[32,16,1408]{2,1,0:T(8,128)(2,1)S(1)} async-done(((bf16[32,16,1408]{2,1,0:T(8,128)(2,1)}), bf16[32,16,1408]{2,1,0:T(8,128)(2,1)S(1)}, u32[]{:S(2)}, u32[]{:S(2)}) %all-to-all-start.2) | async-done | bytes 1441824 | tf_op jit(solution)/shard_map/all_to_all | solution.py:454
  135.1 2.2 %collective-permute-start.7 = (bf16[272,256]{1,0:T(8,128)(2,1)S(1)}, bf16[272,256]{1,0:T(8,128)(2,1)S(1)}, u32[]{:S(2)}, u32[]{:S(2)}) collective-permute-start(bf16[272,256]{1,0:T(8,128)(2,1)S(1)} %get-tuple-element.46), channel_id=1, source_target_pairs={{0,8},{2,10},{4,12},{6,14},{8,0},{10,2},{12,4},{14,6},{1,9},{3,11}... | collective-permute-start | bytes 417800 | tf_op jit(solution)/shard_map/ppermute | solution.py:463
  138.8 2.7 %collective-permute-start.9 = (bf16[272,256]{1,0:T(8,128)(2,1)S(1)}, bf16[272,256]{1,0:T(8,128)(2,1)S(1)}, u32[]{:S(2)}, u32[]{:S(2)}) collective-permute-start(bf16[272,256]{1,0:T(8,128)(2,1)S(1)} %get-tuple-element.48), channel_id=1, source_target_pairs={{0,12},{2,14},{4,0},{6,2},{8,4},{10,6},{12,8},{14,10},{1,13},{3,15... | collective-permute-start | bytes 417800 | tf_op jit(solution)/shard_map/ppermute | solution.py:463
  141.5 3.9 %fusion.3 = bf16[1,128,4096]{2,1,0:T(8,128)(2,1)} fusion(bf16[128,4096]{1,0:T(8,128)(2,1)} %collective-permute-done.12, bf16[320,4096]{1,0:T(8,128)(2,1)} %get-tuple-element.55, f32[320]{0:T(512)S(1)} %slice_reduce_fusion, bf16[320,256]{1,0:T(8,128)(2,1)S(1)} %copy-done.20), kind=kOutput, calls=%fused_computation.10 | convolution fusion | flops 341049344 | bytes 4802560 | tf_op jit(solution)/shard_map/dot_general | solution.py:364
  145.4 3.5 %collective-permute-done.7.p1 = bf16[272,256]{1,0:T(8,128)(2,1)S(1)} collective-permute-done((bf16[272,256]{1,0:T(8,128)(2,1)S(1)}, bf16[272,256]{1,0:T(8,128)(2,1)S(1)}, u32[]{:S(2)}, u32[]{:S(2)}) %collective-permute-start.7) | collective-permute-done | bytes 139296 | tf_op jit(solution)/shard_map/ppermute | solution.py:463
  148.9 3.3 %collective-permute-done.9.p3 = bf16[272,256]{1,0:T(8,128)(2,1)S(1)} collective-permute-done((bf16[272,256]{1,0:T(8,128)(2,1)S(1)}, bf16[272,256]{1,0:T(8,128)(2,1)S(1)}, u32[]{:S(2)}, u32[]{:S(2)}) %collective-permute-start.9) | collective-permute-done | bytes 139296 | tf_op jit(solution)/shard_map/ppermute | solution.py:463
  (68 shorter events, 15.4 us)
Async XLA Ops:
  6.3 8.3 %copy-start.1 = (bf16[256,4096]{1,0:T(8,128)(2,1)S(1)}, bf16[256,4096]{1,0:T(8,128)(2,1)}, u32[]{:S(2)}) copy-start(bf16[256,4096]{1,0:T(8,128)(2,1)} %x_ref.3) | copy-start | bytes 6291460
  6.3 8.3 %copy-start.6 = (bf16[256,256]{1,0:T(8,128)(2,1)S(1)}, bf16[256,256]{1,0:T(8,128)(2,1)}, u32[]{:S(2)}) copy-start(bf16[256,256]{1,0:T(8,128)(2,1)} %get-tuple-element.32.ohm_ref) | copy-start | bytes 393220
  6.3 8.3 %copy-start.7 = (bf16[256,256]{1,0:T(8,128)(2,1)S(1)}, bf16[256,256]{1,0:T(8,128)(2,1)}, u32[]{:S(2)}) copy-start(bf16[256,256]{1,0:T(8,128)(2,1)} %get-tuple-element.33.oht_ref) | copy-start | bytes 393220
  6.4 29.9 %all-to-all-start = ((bf16[16,16,3200]{2,1,0:T(8,128)(2,1)}), bf16[16,16,3200]{2,1,0:T(8,128)(2,1)}, u32[]{:S(2)}, u32[]{:S(2)}) async-start(bf16[16,16,3200]{2,1,0:T(8,128)(2,1)} %bitcast.33), calls=%async_computation | async-start | bytes 3276800 | tf_op jit(solution)/shard_map/all_to_all | solution.py:391
  14.0 38.8 %collective-permute-start.2 = (bf16[4096,128]{1,0:T(8,128)(2,1)}, bf16[4096,128]{1,0:T(8,128)(2,1)}, u32[]{:S(2)}, u32[]{:S(2)}) collective-permute-start(bf16[4096,128]{1,0:T(8,128)(2,1)} %bitcast.38), channel_id=1, source_target_pairs={{0,1},{1,0},{2,3},{3,2},{4,5},{5,4},{6,7},{7,6},{8,9},{9,8},{10,11... | collective-permute-start | bytes 3145736 | tf_op jit(solution)/shard_map/ppermute | solution.py:375
  14.0 38.8 %collective-permute-start.3 = (bf16[4096,128]{1,0:T(8,128)(2,1)}, bf16[4096,128]{1,0:T(8,128)(2,1)}, u32[]{:S(2)}, u32[]{:S(2)}) collective-permute-start(bf16[4096,128]{1,0:T(8,128)(2,1)} %bitcast.36), channel_id=1, source_target_pairs={{0,1},{1,0},{2,3},{3,2},{4,5},{5,4},{6,7},{7,6},{8,9},{9,8},{10,11... | collective-permute-start | bytes 3145736 | tf_op jit(solution)/shard_map/ppermute | solution.py:375
  14.5 36.8 %collective-permute-start.4 = (bf16[128,4096]{1,0:T(8,128)(2,1)}, bf16[128,4096]{1,0:T(8,128)(2,1)S(1)}, u32[]{:S(2)}, u32[]{:S(2)}) collective-permute-start(bf16[128,4096]{1,0:T(8,128)(2,1)} %bitcast.34), channel_id=1, source_target_pairs={{0,1},{1,0},{2,3},{3,2},{4,5},{5,4},{6,7},{7,6},{8,9},{9,8},{10,11... | collective-permute-start | bytes 3145736 | tf_op jit(solution)/shard_map/ppermute | solution.py:375
  36.3 34.3 %all-to-all-start.1 = ((bf16[16,16,3968]{2,1,0:T(8,128)(2,1)}), bf16[16,16,3968]{2,1,0:T(8,128)(2,1)}, u32[]{:S(2)}, u32[]{:S(2)}) async-start(bf16[16,16,3968]{2,1,0:T(8,128)(2,1)} %bitcast.8), calls=%async_computation.1 | async-start | bytes 4063232 | tf_op jit(solution)/shard_map/all_to_all | solution.py:421
  45.4 21.7 %collective-permute-start.1 = (bf16[128,3200]{1,0:T(8,128)(2,1)S(1)}, bf16[128,3200]{1,0:T(8,128)(2,1)}, u32[]{:S(2)}, u32[]{:S(2)}) collective-permute-start(bf16[128,3200]{1,0:T(8,128)(2,1)S(1)} %get-tuple-element.56), channel_id=1, source_target_pairs={{0,14},{2,0},{4,2},{6,4},{8,6},{10,8},{12,10},{14,12},{1,15},{3,1}... | collective-permute-start | bytes 2457608 | tf_op jit(solution)/shard_map/ppermute | solution.py:420
  51.3 19.3 %collective-permute-start = (bf16[128,3200]{1,0:T(8,128)(2,1)S(1)}, bf16[128,3200]{1,0:T(8,128)(2,1)}, u32[]{:S(2)}, u32[]{:S(2)}) collective-permute-start(bf16[128,3200]{1,0:T(8,128)(2,1)S(1)} %get-tuple-element.57), channel_id=1, source_target_pairs={{0,2},{2,4},{4,6},{6,8},{8,10},{10,12},{12,14},{14,0},{1,3},{3,5},... | collective-permute-start | bytes 2457608 | tf_op jit(solution)/shard_map/ppermute | solution.py:419
  80.7 20.6 %collective-permute-start.6 = (bf16[320,1152]{1,0:T(8,128)(2,1)}, bf16[320,1152]{1,0:T(8,128)(2,1)S(1)}, u32[]{:S(2)}, u32[]{:S(2)}) collective-permute-start(bf16[320,1152]{1,0:T(8,128)(2,1)} %get-tuple-element.44), channel_id=1, source_target_pairs={{0,14},{2,0},{4,2},{6,4},{8,6},{10,8},{12,10},{14,12},{1,15},{3,1}... | collective-permute-start | bytes 2211848 | tf_op jit(solution)/shard_map/ppermute | solution.py:445
  85.2 16.2 %collective-permute-start.5 = (bf16[320,1024]{1,0:T(8,128)(2,1)}, bf16[320,1024]{1,0:T(8,128)(2,1)S(1)}, u32[]{:S(2)}, u32[]{:S(2)}) collective-permute-start(bf16[320,1024]{1,0:T(8,128)(2,1)} %get-tuple-element.43), channel_id=1, source_target_pairs={{0,2},{2,4},{4,6},{6,8},{8,10},{10,12},{12,14},{14,0},{1,3},{3,5},... | collective-permute-start | bytes 1966088 | tf_op jit(solution)/shard_map/ppermute | solution.py:444
  89.1 12.3 %copy-start = (bf16[4096,512]{1,0:T(8,128)(2,1)S(1)}, bf16[4096,512]{1,0:T(8,128)(2,1)}, u32[]{:S(2)}) copy-start(bf16[4096,512]{1,0:T(8,128)(2,1)} %pad_maximum_fusion.wcat_ref) | copy-start | bytes 12582916
  89.1 12.3 %copy-start.8 = (bf16[256,128]{1,0:T(8,128)(2,1)S(1)}, bf16[256,128]{1,0:T(8,128)(2,1)}, u32[]{:S(2)}) copy-start(bf16[256,128]{1,0:T(8,128)(2,1)} %get-tuple-element.42.sc_ref) | copy-start | bytes 196612
  89.1 12.3 %copy-start.9 = (s32[3]{0:T(128)S(1)}, s32[3]{0:T(128)}, u32[]{:S(2)}) copy-start(s32[3]{0:T(128)} %pad_add_fusion.s_ref) | copy-start | bytes 40
  89.1 28.3 %collective-permute-start.10 = (bf16[4096,128]{1,0:T(8,128)(2,1)}, bf16[4096,128]{1,0:T(8,128)(2,1)S(1)}, u32[]{:S(2)}, u32[]{:S(2)}) collective-permute-start(bf16[4096,128]{1,0:T(8,128)(2,1)} %convolution_convert_fusion.2), channel_id=1, source_target_pairs={{0,1},{1,0},{2,3},{3,2},{4,5},{5,4},{6,7},{7,6},{8,9},{9,8},{10,11... | collective-permute-start | bytes 3145736 | tf_op jit(solution)/shard_map/ppermute | solution.py:451
  104.8 8.5 %copy-start.20 = (bf16[320,256]{1,0:T(8,128)(2,1)S(1)}, bf16[320,256]{1,0:T(8,128)(2,1)}, u32[]{:S(2)}) copy-start(bf16[320,256]{1,0:T(8,128)(2,1)} %get-tuple-element.53) | copy-start | bytes 491524
  104.8 28.4 %all-to-all-start.2 = ((bf16[32,16,1408]{2,1,0:T(8,128)(2,1)}), bf16[32,16,1408]{2,1,0:T(8,128)(2,1)S(1)}, u32[]{:S(2)}, u32[]{:S(2)}) async-start(bf16[32,16,1408]{2,1,0:T(8,128)(2,1)} %shard_map.130), calls=%async_computation.2 | async-start | bytes 2883584 | tf_op jit(solution)/shard_map/all_to_all | solution.py:454
  113.0 6.4 %collective-permute-start.11 = (bf16[4096,128]{1,0:T(8,128)(2,1)}, bf16[4096,128]{1,0:T(8,128)(2,1)S(1)}, u32[]{:S(2)}, u32[]{:S(2)}) collective-permute-start(bf16[4096,128]{1,0:T(8,128)(2,1)} %convolution_convert_fusion.1), channel_id=1, source_target_pairs={{0,1},{1,0},{2,3},{3,2},{4,5},{5,4},{6,7},{7,6},{8,9},{9,8},{10,11... | collective-permute-start | bytes 3145736 | tf_op jit(solution)/shard_map/ppermute | solution.py:451
  117.0 24.5 %collective-permute-start.12 = (bf16[128,4096]{1,0:T(8,128)(2,1)}, bf16[128,4096]{1,0:T(8,128)(2,1)}, u32[]{:S(2)}, u32[]{:S(2)}) collective-permute-start(bf16[128,4096]{1,0:T(8,128)(2,1)} %convolution_convert_fusion), channel_id=1, source_target_pairs={{0,1},{1,0},{2,3},{3,2},{4,5},{5,4},{6,7},{7,6},{8,9},{9,8},{10,11... | collective-permute-start | bytes 3145736 | tf_op jit(solution)/shard_map/ppermute | solution.py:451
  119.4 13.8 %copy-start.5 = (bf16[4,256,512]{2,1,0:T(8,128)(2,1)S(1)}, bf16[4,256,512]{2,1,0:T(8,128)(2,1)}, u32[]{:S(2)}) copy-start(bf16[4,256,512]{2,1,0:T(8,128)(2,1)} %copy-done.4) | copy-start | bytes 3145732
  135.1 13.8 %collective-permute-start.7 = (bf16[272,256]{1,0:T(8,128)(2,1)S(1)}, bf16[272,256]{1,0:T(8,128)(2,1)S(1)}, u32[]{:S(2)}, u32[]{:S(2)}) collective-permute-start(bf16[272,256]{1,0:T(8,128)(2,1)S(1)} %get-tuple-element.46), channel_id=1, source_target_pairs={{0,8},{2,10},{4,12},{6,14},{8,0},{10,2},{12,4},{14,6},{1,9},{3,11}... | collective-permute-start | bytes 417800 | tf_op jit(solution)/shard_map/ppermute | solution.py:463
  137.3 11.5 %collective-permute-start.8 = (bf16[272,256]{1,0:T(8,128)(2,1)S(1)}, bf16[272,256]{1,0:T(8,128)(2,1)S(1)}, u32[]{:S(2)}, u32[]{:S(2)}) collective-permute-start(bf16[272,256]{1,0:T(8,128)(2,1)S(1)} %get-tuple-element.47), channel_id=1, source_target_pairs={{0,4},{2,6},{4,8},{6,10},{8,12},{10,14},{12,0},{14,2},{1,5},{3,7},... | collective-permute-start | bytes 417800 | tf_op jit(solution)/shard_map/ppermute | solution.py:463
  138.8 13.4 %collective-permute-start.9 = (bf16[272,256]{1,0:T(8,128)(2,1)S(1)}, bf16[272,256]{1,0:T(8,128)(2,1)S(1)}, u32[]{:S(2)}, u32[]{:S(2)}) collective-permute-start(bf16[272,256]{1,0:T(8,128)(2,1)S(1)} %get-tuple-element.48), channel_id=1, source_target_pairs={{0,12},{2,14},{4,0},{6,2},{8,4},{10,6},{12,8},{14,10},{1,13},{3,15... | collective-permute-start | bytes 417800 | tf_op jit(solution)/shard_map/ppermute | solution.py:463
  (13 other events, 78.7 us)
where the time goes:
time: 155 us; the launch traced here: 153 us
  waiting for transfers between devices  57.5 us (37%)
  starting transfers between devices  41.1 us (27%)
  Pallas kernels  24.3 us (16%)
  matrix products  17.7 us (11%)
  other arithmetic  7.06 us (5%)
  local copies, waits for them, and re-layouts  4.38 us (3%)
    dot_general x6, matrix products, tdot(): lax.dot_general(a, b, (((0,), (0,)), ((), ())), preferred_element_type=F32)  17.7 us
    all_to_all x1, waiting for transfers between devices, per_device(): lax.all_to_all(a_send.reshape(16, 16, -1), 'ep', 0, 0, tiled=True)  14.4 us
    all_to_all x1, waiting for transfers between devices, per_device(): r1 = lax.all_to_all(p1, ('ep', 'core'), 0, 0, tiled=True).reshape(512, -1)  11.7 us
    ppermute x1, waiting for transfers between devices, per_device(): z2 = lax.ppermute(a_recv[128:], 'z', around(-1))  10.8 us
    ppermute x1, waiting for transfers between devices, per_device(): up = lax.ppermute(up, 'z', around(1))  10.2 us
    pallas_call x1, Pallas kernels, per_device(): call(expert_kernel, outs, (FAR,) * 6, 63, out_specs=(FAR,) * 8, scratch_s...  10.1 us
    all_to_all x1, starting transfers between devices, per_device(): r1 = lax.all_to_all(p1, ('ep', 'core'), 0, 0, tiled=True).reshape(512, -1)  8.11 us
    all_to_all x1, starting transfers between devices, per_device(): lax.all_to_all(a_send.reshape(16, 16, -1), 'ep', 0, 0, tiled=True)  7.62 us
  transfers between devices with their start and end apart: 16, of which 7 were waited for; matrix products, arithmetic and copies ran while one was open for 17% of the time, Pallas kernels for 6%

commit v1 on v0

--- a/solution.py
+++ b/solution.py
@@ -15,7 +15,14 @@
 B_UNITS = 3
 WHOLE = pl.BlockSpec(memory_space=pltpu.VMEM)
 FAR = pl.BlockSpec(memory_space=pltpu.HBM)
-SCALARS = pl.BlockSpec(memory_space=pltpu.SMEM)
+
+
+def z_index():
+    return lax.axis_index("z")
+
+
+def parity():
+    return lax.rem(z_index(), 2)
 
 
 def iota(shape, dim):
@@ -40,29 +47,33 @@
     return as_bf((iota((256, 128), 0) >> 4) == iota((256, 128), 1))
 
 
-def pack_unit(ohm, oht, src, out):
-    row = iota((256, 256), 0)
+def pack_unit(ohm, oht, fold, src, out):
     out[:, :UNIT] = mm(ohm, src[...]).astype(BF)
-    tail = jnp.zeros((256, 128), F32)
-    for q in range(4):
-        tail += mm(jnp.where(((row >> 2) & 3) == q, oht, jnp.zeros_like(oht)), src[:, q * 128 : q * 128 + 128])
-    out[:, UNIT:WIRE] = tail.astype(BF)
-
-
-def pack_a(s_ref, r_ref, x_ref, g_ref, a_ref, info_ref, ohm_ref, oht_ref, src, dst, sem_in, sem_out):
+    t = mm(oht, src[...]).astype(BF)
+    t = jnp.concatenate([t[:, q * 128 : q * 128 + 128] for q in range(4)], axis=0)
+    out[:, UNIT:WIRE] = mm(fold, t, 0, 0).astype(BF)
+
+
+def pack_a(r_hbm, x_ref, g_ref, a_ref, info_hbm, ohm_hbm, oht_hbm,
+           r_ref, info_ref, ohm_ref, oht_ref, src, dst, sem_in, sem_out):
+    par = parity()
+    get_r = pltpu.make_async_copy(r_hbm, r_ref, sem_in.at[A_UNITS])
+    get_r.start()
+
     def fetch(ref, u):
         return pltpu.make_async_copy(ref.at[:, u * UNIT : (u + 1) * UNIT], src.at[u], sem_in.at[u])
 
     for u in range(A_UNITS):
 
-        @pl.when(s_ref[0] == 0)
+        @pl.when(par == 0)
         def _(u=u):
             fetch(x_ref, u).start()
 
-        @pl.when(s_ref[0] != 0)
+        @pl.when(par != 0)
         def _(u=u):
             fetch(g_ref, u).start()
 
+    get_r.wait()
     r = r_ref[...]
     expert = iota((128, 256), 0)
     named = (r[0:1, :] == expert) | (r[1:2, :] == expert)
@@ -75,14 +86,20 @@
         info_ref[2 * k + 1 : 2 * k + 2, :] = jnp.sum(mine, axis=0, keepdims=True)
     info_ref[4:8, :] = jnp.zeros((4, 256), F32)
     spread = mm(expert_rows(), jnp.where(named, rank, -1.0).astype(BF)).astype(I32)
-    first = s_ref[1] * 20
+    first = lax.axis_index("core") * 20
     ohm_ref[...] = as_bf(spread == first + (ti & 15))
-    oht_ref[...] = as_bf(spread == first + 16 + (ti & 3))
-
+    row64 = iota((64, 128), 0)
+    by_expert = jnp.where(named, rank, -1.0).astype(BF)
+    tail_spread = mm(as_bf((row64 >> 2) == iota((64, 128), 1)), by_expert).astype(I32)
+    oht_ref[...] = as_bf(tail_spread == first + 16 + (iota((64, 256), 0) & 3))
+    fold = fold_matrix()
     outs = []
+    for n, (ref, hbm) in enumerate(((info_ref, info_hbm), (ohm_ref, ohm_hbm), (oht_ref, oht_hbm))):
+        outs.append(pltpu.make_async_copy(ref, hbm, sem_out.at[A_UNITS + n]))
+        outs[-1].start()
     for u in range(A_UNITS):
         fetch(x_ref, u).wait()
-        pack_unit(ohm_ref[...], oht_ref[...], src.at[u], dst.at[u])
+        pack_unit(ohm_ref[...], oht_ref[...], fold, src.at[u], dst.at[u])
         out = pltpu.make_async_copy(dst.at[u], a_ref.at[:, u * WIRE : (u + 1) * WIRE], sem_out.at[u])
         out.start()
         outs.append(out)
@@ -93,8 +110,9 @@
 def pack_b(r_ref, gg_ref, ig_ref, info_ref, ohm_ref, oht_ref, x_ref, g_ref, bx_ref, bg_ref, wt_ref, mask_ref):
     ohm = ohm_ref[...]
     oht = oht_ref[...]
-    pack_unit(ohm, oht, x_ref, bx_ref)
-    pack_unit(ohm, oht, g_ref, bg_ref)
+    fold = fold_matrix()
+    pack_unit(ohm, oht, fold, x_ref, bx_ref)
+    pack_unit(ohm, oht, fold, g_ref, bg_ref)
 
     @pl.when(pl.program_id(0) == 0)
     def _():
@@ -105,14 +123,16 @@
         hi = w.astype(BF)
         lo = (w - hi.astype(F32)).astype(BF)
 
-        def picked(oh, part):
-            return jnp.sum(oh.astype(F32) * mm(expert_rows(), part), axis=1, keepdims=True)
+        def picked(oh, rows, part):
+            return jnp.sum(oh.astype(F32) * mm(rows, part), axis=1, keepdims=True)
 
         lane = iota((256, 128), 1)
-        vals = jnp.where(lane == 0, picked(ohm, hi), 0.0)
-        vals = jnp.where(lane == 1, picked(ohm, lo), vals)
-        vals = jnp.where(lane == 2, picked(oht, hi), vals)
-        vals = jnp.where(lane == 3, picked(oht, lo), vals)
+        lane64 = iota((64, 128), 1)
+        rows64 = as_bf((iota((64, 128), 0) >> 2) == lane64)
+        tails = jnp.where(lane64 == 2, picked(oht, rows64, hi), 0.0)
+        tails = jnp.where(lane64 == 3, picked(oht, rows64, lo), tails).astype(BF)
+        vals = jnp.where(lane == 0, picked(ohm, expert_rows(), hi), mm(fold[0:64, :], tails, 0, 0))
+        vals = jnp.where(lane == 1, picked(ohm, expert_rows(), lo), vals)
         wt_ref[...] = vals.astype(BF)
 
         eye = as_bf(iota((256, 256), 0) == iota((256, 256), 1))
@@ -133,17 +153,21 @@
     return slice(u * UNIT, (u + 1) * UNIT)
 
 
+def place_tail(dst, u, t):
+    for q in range(4):
+        dst[256:320, u * UNIT + q * 128 : u * UNIT + q * 128 + 128] = t[q * 64 : q * 64 + 64, :]
+
+
 def unpack(fold, buf, dst, u):
     dst[0:256, cols(u)] = buf[:, 0:UNIT]
-    t = mm(fold, buf[:, UNIT:WIRE]).astype(BF)
-    for q in range(4):
-        dst[256:320, u * UNIT + q * 128 : u * UNIT + q * 128 + 128] = t[q * 64 : q * 64 + 64, :]
-
-
-def expert_kernel(s_ref, a_ref, z1_ref, z2_ref, b_ref, wcat_ref, wd_hbm,
-                  x_hbm, g_hbm, c_hbm, hid_hbm, in_hbm, sc_hbm, up_hbm, dn_hbm,
+    place_tail(dst, u, mm(fold, buf[:, UNIT:WIRE]).astype(BF))
+
+
+def expert_kernel(a_ref, z1_ref, z2_ref, b_ref, wcat_ref, wd_hbm,
+                  c_hbm, hid_hbm, in_hbm, sc_hbm, up_hbm, dn_hbm,
                   buf_a, buf_z, buf_b, wt_buf, wc, wd, xv, gv, pre_acc, gh_acc,
                   c_out, hid_out, in_out, sc_out, up_out, dn_out, sem_i, sem_w, sem_o):
+    par = parity()
     units = A_UNITS + B_UNITS
     at = 2 * B_UNITS * WIRE
     in_wt = pltpu.make_async_copy(b_ref.at[:, at : at + 128], wt_buf, sem_w.at[2 * units])
@@ -184,12 +208,12 @@
             copy.wait()
         if u < A_UNITS:
 
-            @pl.when(s_ref[0] == 0)
+            @pl.when(par == 0)
             def _(u=u):
                 unpack(fold, buf_a.at[u], xv, u)
                 unpack(fold, buf_z.at[u], gv, u)
 
-            @pl.when(s_ref[0] != 0)
+            @pl.when(par != 0)
             def _(u=u):
                 unpack(fold, buf_a.at[u], gv, u)
                 unpack(fold, buf_z.at[u], xv, u)
@@ -200,8 +224,6 @@
             copy.wait()
         if u % 2 == 1:
             both = slice((u - 1) * UNIT, (u + 1) * UNIT)
-            send(xv.at[:, both], x_hbm.at[:, both])
-            send(gv.at[:, both], g_hbm.at[:, both])
             p = mm(xv[:, both], wc[both, :])
             g = mm(gv[:, both], wd[:, both], 1, 1)
             if u > 1:
@@ -250,7 +272,7 @@
     for i in range(4):
         dst = up_out if i < 2 else dn_out
         for c in range(2):
-            at = pl.multiple_of((2 * i + 1 - s_ref[0]) * 512 + c * 256, 256)
+            at = pl.multiple_of((2 * i + 1 - par) * 512 + c * 256, 256)
             col = (i % 2) * 512 + c * 256
             dst[:, col : col + 256] = mm(ins, wc[pl.ds(at, 256), :], 1, 1).astype(BF)
         if i == 1:
@@ -260,7 +282,35 @@
         copy.wait()
 
 
-def return_kernel(s_ref, in_ref, wcat_ref, sc_ref, up_ref, dn_ref, out_ref):
+def rows_kernel(a_ref, z1_ref, z2_ref, b_ref, x_out, g_out):
+    par = parity()
+    fold = fold_matrix()
+
+    def from_z(dst, u):
+        dst[0:128, cols(u)] = z1_ref[:, u * WIRE : u * WIRE + UNIT]
+        dst[128:256, cols(u)] = z2_ref[:, u * WIRE : u * WIRE + UNIT]
+        at = slice(u * WIRE + UNIT, (u + 1) * WIRE)
+        place_tail(dst, u, mm(fold, jnp.concatenate([z1_ref[:, at], z2_ref[:, at]], axis=0)).astype(BF))
+
+    @pl.when(par == 0)
+    def _():
+        for u in range(A_UNITS):
+            unpack(fold, a_ref.at[:, wire(u)], x_out, u)
+            from_z(g_out, u)
+
+    @pl.when(par != 0)
+    def _():
+        for u in range(A_UNITS):
+            unpack(fold, a_ref.at[:, wire(u)], g_out, u)
+            from_z(x_out, u)
+
+    for n in range(B_UNITS):
+        unpack(fold, b_ref.at[:, wire(n)], x_out, A_UNITS + n)
+        unpack(fold, b_ref.at[:, wire(B_UNITS + n)], g_out, A_UNITS + n)
+
+
+def return_kernel(in_ref, wcat_ref, sc_ref, up_ref, dn_ref, out_ref):
+    par = parity()
     fold = fold_matrix()
     ins = in_ref[...]
     lane = iota((256, 128), 1)
@@ -273,7 +323,7 @@
             src = (up_ref, dn_ref)[u]
             tails = []
             for h in range(2):
-                at = pl.multiple_of((4 * u + 2 * h + s_ref[0]) * 512 + c * 256, 256)
+                at = pl.multiple_of((4 * u + 2 * h + par) * 512 + c * 256, 256)
                 col = h * 512 + c * 256
                 part = mm(ins, wcat_ref[pl.ds(at, 256), :], 1, 1) + src[0:320, col : col + 256].astype(F32)
                 part = part.astype(BF)
@@ -287,7 +337,7 @@
             out_ref[2 * b + c, :, 2 * WIRE :] = vals[16 * b : 16 * b + 16, :]
 
 
-def combine_kernel(s_ref, mask_ref, r1_ref, *outs):
+def combine_kernel(mask_ref, r1_ref, *outs):
     acc_ref = outs[4]
     slot = iota((256, 512), 1)
     zero = jnp.zeros((256, 512), BF)
@@ -315,7 +365,7 @@
         scores = jnp.where(row16 == n, rows[n], scores)
     scores = scores.astype(BF)
     for n in range(4):
-        dest = lax.rem(s_ref[2] + 2 * n, 8)
+        dest = lax.rem(z_index() + 2 * n, 8)
         at = pl.multiple_of((dest >> 1) * 256, 256)
         outs[n][0:256, :] = acc_ref[:, pl.ds(at, 256)]
         outs[n][256:272, :] = scores
@@ -336,12 +386,11 @@
     return jax.ShapeDtypeStruct(shape, dtype)
 
 
-def call(kernel, outs, ins, mib, scalars=True, out_specs=None, **kw):
-    specs = ([SCALARS] if scalars else []) + list(ins)
+def call(kernel, outs, ins, mib, out_specs=None, **kw):
     return pl.pallas_call(
         kernel,
         out_shape=outs,
-        in_specs=specs,
+        in_specs=list(ins),
         out_specs=out_specs or jax.tree.map(lambda _: WHOLE, outs),
         compiler_params=pltpu.CompilerParams(vmem_limit_bytes=mib * 2**20),
         **kw,
@@ -365,8 +414,6 @@
 
 
 def per_device(tokens, cotangent, routing, group_gate, inner_gate, w_gate, w_up, w_down):
-    z = lax.axis_index("z")
-    info = jnp.stack([z % 2, lax.axis_index("core"), z]).astype(I32)
     gg = group_gate[None, :]
     ig = inner_gate.T
     rt = routing.T
@@ -380,14 +427,15 @@
     small = pltpu.CompilerParams(vmem_limit_bytes=12 * 2**20)
     a_send, ranks, ohm, oht = call(
         pack_a,
-        (sds((256, A_UNITS * WIRE)), sds((8, 256), F32), sds((256, 256)), sds((256, 256))),
-        (WHOLE, FAR, FAR),
+        (sds((256, A_UNITS * WIRE)), sds((8, 256), F32), sds((256, 256)), sds((64, 256))),
+        (FAR,) * 3,
         63,
-        out_specs=(FAR, WHOLE, WHOLE, WHOLE),
+        out_specs=(FAR,) * 4,
         scratch_shapes=[
-            vmem(A_UNITS, 256, UNIT), vmem(A_UNITS, 256, WIRE), sems(A_UNITS), sems(A_UNITS),
+            pltpu.VMEM((2, 256), I32), pltpu.VMEM((8, 256), F32), vmem(256, 256), vmem(64, 256),
+            vmem(A_UNITS, 256, UNIT), vmem(A_UNITS, 256, WIRE), sems(A_UNITS + 1), sems(A_UNITS + 3),
         ],
-    )(info, rt, tokens, cotangent)
+    )(rt, tokens, cotangent)
     a_recv = lax.all_to_all(a_send.reshape(16, 16, -1), "ep", 0, 0, tiled=True).reshape(256, -1)
 
     bx, bg, wt, masks = pl.pallas_call(
@@ -399,7 +447,7 @@
             pl.BlockSpec((2, 256), whole),
             pl.BlockSpec((8, 256), whole),
             pl.BlockSpec((256, 256), whole),
-            pl.BlockSpec((256, 256), whole),
+            pl.BlockSpec((64, 256), whole),
             pl.BlockSpec((256, UNIT), later),
             pl.BlockSpec((256, UNIT), later),
         ],
@@ -423,26 +471,27 @@
     wd = jnp.concatenate([w_down[0], other[2]], axis=0)
 
     outs = (
-        sds((320, 4096)), sds((320, 4096)), sds((320, 128), F32), sds((320, 256)),
-        sds((320, 512)), sds((256, 128)), sds((320, 1024)), sds((320, 1152)),
+        sds((320, 128), F32), sds((320, 256)), sds((320, 512)), sds((256, 128)), sds((320, 1024)), sds((320, 1152)),
     )
     n = A_UNITS + B_UNITS
-    xs, gs, cw, hid, ins, sc, up, dn = call(
+    cw, hid, ins, sc, up, dn = call(
         expert_kernel,
         outs,
         (FAR,) * 6,
         63,
-        out_specs=(FAR,) * 8,
+        out_specs=(FAR,) * 6,
         scratch_shapes=[
             vmem(A_UNITS, 256, WIRE), vmem(A_UNITS, 256, WIRE), vmem(2 * B_UNITS, 256, WIRE), vmem(256, 128),
             vmem(4096, 512), vmem(256, 4096), vmem(320, 4096), vmem(320, 4096),
             pltpu.VMEM((320, 512), F32), pltpu.VMEM((320, 256), F32),
             pltpu.VMEM((320, 128), F32), vmem(320, 256), vmem(320, 512), vmem(256, 128),
-            vmem(320, 1024), vmem(320, 1152), sems(3 * n), sems(2 * n + 1), sems(n + 6),
+            vmem(320, 1024), vmem(320, 1152), sems(3 * n), sems(2 * n + 1), sems(6),
         ],
-    )(info, a_recv, z1, z2, b_recv, wcat, wd)
+    )(a_recv, z1, z2, b_recv, wcat, wd)
     up = lax.ppermute(up, "z", around(1))
     dn = lax.ppermute(dn, "z", around(-1))
+
+    xs, gs = call(rows_kernel, (sds((320, 4096)),) * 2, (WHOLE,) * 4, 50)(a_recv, z1, z2, b_recv)
 
     scaled = (cw[:, 0:1] * gs).astype(BF)
     d_par = tdot(hid[:, 128:], scaled).astype(BF)
@@ -450,7 +499,7 @@
     u_par = tdot(xs, ins[:, 384:512]).astype(BF)
     d_par, g_par, u_par = [lax.ppermute(t, "core", swap) for t in (d_par, g_par, u_par)]
 
-    p1 = call(return_kernel, sds((32, 16, 2 * WIRE + 128)), (WHOLE,) * 5, 8)(info, ins, wcat, sc, up, dn)
+    p1 = call(return_kernel, sds((32, 16, 2 * WIRE + 128)), (WHOLE,) * 5, 8)(ins, wcat, sc, up, dn)
     r1 = lax.all_to_all(p1, ("ep", "core"), 0, 0, tiled=True).reshape(512, -1)
 
     down_grad = (tdot(hid[:, :128], scaled) + d_par).astype(BF)
@@ -459,10 +508,10 @@
 
     pieces = call(
         combine_kernel, (sds((272, 256)),) * 4, (WHOLE,) * 2, 8, scratch_shapes=[pltpu.VMEM((256, 1024), BF)]
-    )(info, masks, r1)
+    )(masks, r1)
     got = [lax.ppermute(pieces[n], "z", around(2 * n)) for n in (2, 1, 3)]
     token_grad, group_grad, inner_grad = call(
-        final_kernel, (sds((256, 256)), sds((1, 256), F32), sds((2, 256), F32)), (WHOLE,) * 6, 4, scalars=False
+        final_kernel, (sds((256, 256)), sds((1, 256), F32), sds((2, 256), F32)), (WHOLE,) * 6, 4
     )(gg, ig, pieces[0], *got)
     return token_grad, group_grad[0], inner_grad.T, gate_grad[None], upper_grad[None], down_grad[None]
 

time: 155 us -> 151 us (0.974)
  waiting for transfers between devices: 57.5 us -> 44.8 us
  local copies, waits for them, and re-layouts: 4.38 us -> 7.05 us
  Pallas kernels: 24.3 us -> 26.9 us
  starting transfers between devices: 41.1 us -> 42.7 us
    ppermute x1, waiting for transfers between devices: 10.8 us -> 0.01 us  [per_device(): z2 = lax.ppermute(a_recv[128:], 'z', around(-1))]
    ppermute x1, waiting for transfers between devices: 10.2 us -> 1.77 us  [per_device(): up = lax.ppermute(up, 'z', around(1))]
    ppermute x1, waiting for transfers between devices: 3.52 us -> 9.59 us  [per_device(): z1 = lax.ppermute(a_recv[:128], 'z', around(1))]
    pallas_call x1 -> x2, Pallas kernels: 10.1 us -> 14.7 us  [the longest x1 9.34 us: per_device(): call(expert_kernel, outs, (FAR,) * 6, 63, out_specs=(FAR,) * 6, scratch_s...]
    unnamed x42, local copies, waits for them, and re-layouts: 2.65 us -> 6.79 us
    all_to_all x1, waiting for transfers between devices: 0.01 us -> 2.78 us  [per_device(): lax.all_to_all(b_send.reshape(16, 16, -1), 'ep', 0, 0, tiled=True)]
    ppermute x1, starting transfers between devices: 0.01 us -> 1.99 us  [per_device(): z1 = lax.ppermute(a_recv[:128], 'z', around(1))]
    ppermute x1, starting transfers between devices: 5.92 us -> 4.03 us  [per_device(): z2 = lax.ppermute(a_recv[128:], 'z', around(-1))]
  transfers between devices with their start and end apart: 16 -> 16, of which waited for: 7 -> 7; matrix products, arithmetic and copies ran while one was open for 17% -> 18% of each run, Pallas kernels for 6% -> 8%
where the time goes in v1:
time: 151 us; the launch traced here: 150 us
  waiting for transfers between devices  44.8 us (30%)
  starting transfers between devices  42.7 us (28%)
  Pallas kernels  26.9 us (18%)
  matrix products  19 us (13%)
  other arithmetic  8.39 us (6%)
  local copies, waits for them, and re-layouts  7.05 us (5%)
    dot_general x6, matrix products, tdot(): lax.dot_general(a, b, (((0,), (0,)), ((), ())), preferred_element_type=F32)  19 us
    all_to_all x1, waiting for transfers between devices, per_device(): lax.all_to_all(a_send.reshape(16, 16, -1), 'ep', 0, 0, tiled=True)  12.8 us
    all_to_all x1, waiting for transfers between devices, per_device(): r1 = lax.all_to_all(p1, ('ep', 'core'), 0, 0, tiled=True).reshape(512, -1)  10.9 us
    ppermute x1, waiting for transfers between devices, per_device(): z1 = lax.ppermute(a_recv[:128], 'z', around(1))  9.59 us
    pallas_call x1, Pallas kernels, per_device(): call(expert_kernel, outs, (FAR,) * 6, 63, out_specs=(FAR,) * 6, scratch_s...  9.34 us
    all_to_all x1, starting transfers between devices, per_device(): r1 = lax.all_to_all(p1, ('ep', 'core'), 0, 0, tiled=True).reshape(512, -1)  8.12 us
    all_to_all x1, starting transfers between devices, per_device(): lax.all_to_all(a_send.reshape(16, 16, -1), 'ep', 0, 0, tiled=True)  7.62 us
    all_to_all x1, starting transfers between devices, per_device(): lax.all_to_all(b_send.reshape(16, 16, -1), 'ep', 0, 0, tiled=True)  7.41 us
  transfers between devices with their start and end apart: 16, of which 7 were waited for; matrix products, arithmetic and copies ran while one was open for 18% of the time, Pallas kernels for 8%

profile of v1, /device:TPU:2, one launch (start us, length us, event | category | flops | bytes accessed | tf_op | source)
XLA Modules:
  0.0 149.6 jit_solution(13753634675230863975)
XLA Ops:
  0.6 4.3 %shard_map.127 = (bf16[256,3200]{1,0:T(8,128)(2,1)}, f32[8,256]{1,0:T(8,128)}, bf16[256,256]{1,0:T(8,128)(2,1)}, bf16[64,256]{1,0:T(8,128)(2,1)}) custom-call(s32[2,256]{1,0:T(2,128)} %bitcast.27, bf16[256,4096]{1,0:T(8,128)(2,1)} %x_ref.3, bf16[256,4096]{1,0:T(8,128)(2,1)} %g_ref.3), custom_call_target="tpu_custom_call" | custom-call | tf_op jit(solution)/shard_map/pallas_call | solution.py:428
  5.0 7.6 %all-to-all-start = ((bf16[16,16,3200]{2,1,0:T(8,128)(2,1)}), bf16[16,16,3200]{2,1,0:T(8,128)(2,1)S(1)}, u32[]{:S(2)}, u32[]{:S(2)}) async-start(bf16[16,16,3200]{2,1,0:T(8,128)(2,1)} %bitcast.34), calls=%async_computation | async-start | bytes 3276800 | tf_op jit(solution)/shard_map/all_to_all | solution.py:439
  16.5 3.0 %shard_map.128 = (bf16[256,1920]{1,0:T(8,128)(2,1)S(1)}, bf16[256,1920]{1,0:T(8,128)(2,1)S(1)}, bf16[256,128]{1,0:T(8,128)(2,1)S(1)}, bf16[4,256,512]{2,1,0:T(8,128)(2,1)S(1)}) custom-call(s32[2,256]{1,0:T(2,128)S(1)} %bitcast.28, f32[1,256]{1,0:T(1,128)S(1)} %bitcast.31, f32[2,256]{1,0:T(2,128)S(1)} %bitcast.29, f32[8,256]{1,0:T(8,128)S(1)} %copy-done.13, ...), custom_call_target="tpu_custom_call" | custom-call | tf_op jit(solution)/shard_map/pallas_call | solution.py:441
  22.0 12.8 %all-to-all-done = bf16[16,16,3200]{2,1,0:T(8,128)(2,1)S(1)} async-done(((bf16[16,16,3200]{2,1,0:T(8,128)(2,1)}), bf16[16,16,3200]{2,1,0:T(8,128)(2,1)S(1)}, u32[]{:S(2)}, u32[]{:S(2)}) %all-to-all-start) | async-done | bytes 1638432 | tf_op jit(solution)/shard_map/all_to_all | solution.py:439
  34.8 7.4 %all-to-all-start.1 = ((bf16[16,16,3968]{2,1,0:T(8,128)(2,1)}), bf16[16,16,3968]{2,1,0:T(8,128)(2,1)}, u32[]{:S(2)}, u32[]{:S(2)}) async-start(bf16[16,16,3968]{2,1,0:T(8,128)(2,1)} %bitcast.33), calls=%async_computation.1 | async-start | bytes 4063232 | tf_op jit(solution)/shard_map/all_to_all | solution.py:469
  44.4 4.0 %collective-permute-start.1 = (bf16[128,3200]{1,0:T(8,128)(2,1)S(1)}, bf16[128,3200]{1,0:T(8,128)(2,1)}, u32[]{:S(2)}, u32[]{:S(2)}) collective-permute-start(bf16[128,3200]{1,0:T(8,128)(2,1)S(1)} %get-tuple-element.56), channel_id=1, source_target_pairs={{0,14},{2,0},{4,2},{6,4},{8,6},{10,8},{12,10},{14,12},{1,15},{3,1}... | collective-permute-start | bytes 2457608 | tf_op jit(solution)/shard_map/ppermute | solution.py:468
  48.4 3.1 %pad_maximum_fusion.1.wd_hbm = bf16[256,4096]{1,0:T(8,128)(2,1)} fusion(bf16[128,4096]{1,0:T(8,128)(2,1)} %collective-permute-done.4, bf16[128,4096]{1,0:T(8,128)(2,1)} %bitcast.9), kind=kLoop, calls=%fused_computation.14 | loop fusion | flops 4194304 | bytes 4194304 | tf_op jit(solution)/shard_map/concatenate | solution.py:471
  51.6 3.7 %pad_maximum_fusion.wcat_ref = bf16[4096,512]{1,0:T(8,128)(2,1)} fusion(bf16[4096,128]{1,0:T(8,128)(2,1)} %collective-permute-done.3, bf16[4096,128]{1,0:T(8,128)(2,1)} %bitcast.8, bf16[4096,128]{1,0:T(8,128)(2,1)} %collective-permute-done.2, bf16[4096,128]{1,0:T(8,128)(2,1)} %bitcast.7), kind=kLoop, calls=%fused_computation.13 | loop fusion | flops 16777216 | bytes 8388608 | tf_op jit(solution)/shard_map/concatenate | solution.py:470
  55.3 9.6 %collective-permute-done.z1_ref = bf16[128,3200]{1,0:T(8,128)(2,1)S(1)} collective-permute-done((bf16[128,3200]{1,0:T(8,128)(2,1)S(1)}, bf16[128,3200]{1,0:T(8,128)(2,1)S(1)}, u32[]{:S(2)}, u32[]{:S(2)}) %collective-permute-start) | collective-permute-done | bytes 819232 | tf_op jit(solution)/shard_map/ppermute | solution.py:467
  64.9 2.8 %all-to-all-done.1 = bf16[16,16,3968]{2,1,0:T(8,128)(2,1)} async-done(((bf16[16,16,3968]{2,1,0:T(8,128)(2,1)}), bf16[16,16,3968]{2,1,0:T(8,128)(2,1)}, u32[]{:S(2)}, u32[]{:S(2)}) %all-to-all-start.1) | async-done | bytes 2031648 | tf_op jit(solution)/shard_map/all_to_all | solution.py:469
  67.7 9.3 %shard_map.129 = (f32[320,128]{1,0:T(8,128)}, bf16[320,256]{1,0:T(8,128)(2,1)}, bf16[320,512]{1,0:T(8,128)(2,1)}, bf16[256,128]{1,0:T(8,128)(2,1)}, bf16[320,102...) custom-call(bf16[256,3200]{1,0:T(8,128)(2,1)} %bitcast.24, bf16[128,3200]{1,0:T(8,128)(2,1)} %copy-done.5, ...), custom_call_target="tpu_custom_call" | custom-call | tf_op jit(solution)/shard_map/pallas_call | solution.py:477
  77.0 5.9 %collective-permute-start.6 = (bf16[320,1152]{1,0:T(8,128)(2,1)}, bf16[320,1152]{1,0:T(8,128)(2,1)S(1)}, u32[]{:S(2)}, u32[]{:S(2)}) collective-permute-start(bf16[320,1152]{1,0:T(8,128)(2,1)} %get-tuple-element.44), channel_id=1, source_target_pairs={{0,14},{2,0},{4,2},{6,4},{8,6},{10,8},{12,10},{14,12},{1,15},{3,1}... | collective-permute-start | bytes 2211848 | tf_op jit(solution)/shard_map/ppermute | solution.py:492
  85.5 5.4 %shard_map.133 = (bf16[320,4096]{1,0:T(8,128)(2,1)}, bf16[320,4096]{1,0:T(8,128)(2,1)}) custom-call(bf16[256,3200]{1,0:T(8,128)(2,1)S(1)} %bitcast.25, bf16[128,3200]{1,0:T(8,128)(2,1)S(1)} %copy-done.6, bf16[128,3200]{1,0:T(8,128)(2,1)} %collective-permute-done.1.z2_ref, bf16[256,3968]{1,0:T(8,128)(2,1)} %bitcast.6.b_ref), custom_call_target="tpu_custom_call" | custom-call | tf_op jit(solution)/shard_map/pallas_call | solution.py:494
  90.9 3.9 %convolution_convert_fusion.2 = bf16[4096,128]{1,0:T(8,128)(2,1)} fusion(bf16[320,4096]{1,0:T(8,128)(2,1)} %get-tuple-element.52, bf16[320,512]{1,0:T(8,128)(2,1)S(1)} %copy-done.7), kind=kOutput, calls=%fused_computation.9 | convolution fusion | flops 336068608 | bytes 3751936 | tf_op jit(solution)/shard_map/dot_general | solution.py:413
  99.2 2.8 %shard_map.130 = bf16[32,16,1408]{2,1,0:T(8,128)(2,1)} custom-call(bf16[320,512]{1,0:T(8,128)(2,1)S(1)} %copy-done.7, bf16[4096,512]{1,0:T(8,128)(2,1)S(1)} %copy-done, bf16[256,128]{1,0:T(8,128)(2,1)S(1)} %copy-done.11, bf16[320,1024]{1,0:T(8,128)(2,1)S(1)} %collective-permute-done.5.up_ref, bf16[320,1152]{1,0:T(8,128)(2,1)S(1)} %collective-permute-done.6.dn_ref), custom_call_target="tpu_custom_call" | custom-call | tf_op jit(solution)/shard_map/pallas_call | solution.py:502
  102.0 8.1 %all-to-all-start.2 = ((bf16[32,16,1408]{2,1,0:T(8,128)(2,1)}), bf16[32,16,1408]{2,1,0:T(8,128)(2,1)S(1)}, u32[]{:S(2)}, u32[]{:S(2)}) async-start(bf16[32,16,1408]{2,1,0:T(8,128)(2,1)} %shard_map.130), calls=%async_computation.2 | async-start | bytes 2883584 | tf_op jit(solution)/shard_map/all_to_all | solution.py:503
  110.3 3.7 %convolution_convert_fusion = bf16[128,4096]{1,0:T(8,128)(2,1)} fusion(bf16[320,4096]{1,0:T(8,128)(2,1)} %get-tuple-element.55, f32[320]{0:T(512)S(1)} %slice_reduce_fusion, bf16[320,256]{1,0:T(8,128)(2,1)S(1)} %copy-done.20), kind=kOutput, calls=%fused_computation.7 | convolution fusion | flops 340000768 | bytes 3753984 | tf_op jit(solution)/shard_map/dot_general | solution.py:413
  116.2 3.4 %fusion.4 = bf16[1,4096,128]{2,1,0:T(8,128)(2,1)} fusion(bf16[320,4096]{1,0:T(8,128)(2,1)S(1)} %copy-done.18, bf16[4096,128]{1,0:T(8,128)(2,1)} %collective-permute-done.11, bf16[320,512]{1,0:T(8,128)(2,1)S(1)} %copy-done.7), kind=kOutput, calls=%fused_computation.11 | convolution fusion | flops 337117184 | bytes 4800512 | tf_op jit(solution)/shard_map/dot_general | solution.py:413
  119.6 10.9 %all-to-all-done.2 = bf16[32,16,1408]{2,1,0:T(8,128)(2,1)S(1)} async-done(((bf16[32,16,1408]{2,1,0:T(8,128)(2,1)}), bf16[32,16,1408]{2,1,0:T(8,128)(2,1)S(1)}, u32[]{:S(2)}, u32[]{:S(2)}) %all-to-all-start.2) | async-done | bytes 1441824 | tf_op jit(solution)/shard_map/all_to_all | solution.py:503
  131.8 2.2 %collective-permute-start.7 = (bf16[272,256]{1,0:T(8,128)(2,1)S(1)}, bf16[272,256]{1,0:T(8,128)(2,1)S(1)}, u32[]{:S(2)}, u32[]{:S(2)}) collective-permute-start(bf16[272,256]{1,0:T(8,128)(2,1)S(1)} %get-tuple-element.46), channel_id=1, source_target_pairs={{0,8},{2,10},{4,12},{6,14},{8,0},{10,2},{12,4},{14,6},{1,9},{3,11}... | collective-permute-start | bytes 417800 | tf_op jit(solution)/shard_map/ppermute | solution.py:512
  135.5 2.7 %collective-permute-start.9 = (bf16[272,256]{1,0:T(8,128)(2,1)S(1)}, bf16[272,256]{1,0:T(8,128)(2,1)S(1)}, u32[]{:S(2)}, u32[]{:S(2)}) collective-permute-start(bf16[272,256]{1,0:T(8,128)(2,1)S(1)} %get-tuple-element.48), channel_id=1, source_target_pairs={{0,12},{2,14},{4,0},{6,2},{8,4},{10,6},{12,8},{14,10},{1,13},{3,15... | collective-permute-start | bytes 417800 | tf_op jit(solution)/shard_map/ppermute | solution.py:512
  138.1 3.9 %fusion.3 = bf16[1,128,4096]{2,1,0:T(8,128)(2,1)} fusion(bf16[128,4096]{1,0:T(8,128)(2,1)} %collective-permute-done.12, bf16[320,4096]{1,0:T(8,128)(2,1)} %get-tuple-element.55, f32[320]{0:T(512)S(1)} %slice_reduce_fusion, bf16[320,256]{1,0:T(8,128)(2,1)S(1)} %copy-done.20), kind=kOutput, calls=%fused_computation.10 | convolution fusion | flops 341049344 | bytes 4802560 | tf_op jit(solution)/shard_map/dot_general | solution.py:413
  142.0 3.6 %collective-permute-done.7.p1 = bf16[272,256]{1,0:T(8,128)(2,1)S(1)} collective-permute-done((bf16[272,256]{1,0:T(8,128)(2,1)S(1)}, bf16[272,256]{1,0:T(8,128)(2,1)S(1)}, u32[]{:S(2)}, u32[]{:S(2)}) %collective-permute-start.7) | collective-permute-done | bytes 139296 | tf_op jit(solution)/shard_map/ppermute | solution.py:512
  145.6 3.4 %collective-permute-done.9.p3 = bf16[272,256]{1,0:T(8,128)(2,1)S(1)} collective-permute-done((bf16[272,256]{1,0:T(8,128)(2,1)S(1)}, bf16[272,256]{1,0:T(8,128)(2,1)S(1)}, u32[]{:S(2)}, u32[]{:S(2)}) %collective-permute-start.9) | collective-permute-done | bytes 139296 | tf_op jit(solution)/shard_map/ppermute | solution.py:512
  (68 shorter events, 21.2 us)
Async XLA Ops:
  4.9 8.3 %copy-start.10 = (bf16[256,256]{1,0:T(8,128)(2,1)S(1)}, bf16[256,256]{1,0:T(8,128)(2,1)}, u32[]{:S(2)}) copy-start(bf16[256,256]{1,0:T(8,128)(2,1)} %get-tuple-element.32.ohm_ref) | copy-start | bytes 393220
  4.9 8.3 %copy-start.12 = (bf16[64,256]{1,0:T(8,128)(2,1)S(1)}, bf16[64,256]{1,0:T(8,128)(2,1)}, u32[]{:S(2)}) copy-start(bf16[64,256]{1,0:T(8,128)(2,1)} %get-tuple-element.33.oht_ref) | copy-start | bytes 98308
  5.0 8.3 %copy-start.13 = (f32[8,256]{1,0:T(8,128)S(1)}, f32[8,256]{1,0:T(8,128)}, u32[]{:S(2)}) copy-start(f32[8,256]{1,0:T(8,128)} %get-tuple-element.31.info_ref) | copy-start | bytes 24580
  5.0 8.3 %copy-start.14 = (s32[256,2]{0,1:T(2,128)S(1)}, s32[256,2]{0,1:T(2,128)}, u32[]{:S(2)}) copy-start(s32[256,2]{0,1:T(2,128)} %param.10) | copy-start | bytes 6148
  5.0 8.3 %copy-start.15 = (f32[256,2]{0,1:T(2,128)S(1)}, f32[256,2]{0,1:T(2,128)}, u32[]{:S(2)}) copy-start(f32[256,2]{0,1:T(2,128)} %param.12) | copy-start | bytes 6148
  5.0 8.3 %copy-start.16 = (f32[256]{0:T(256)S(1)}, f32[256]{0:T(256)}, u32[]{:S(2)}) copy-start(f32[256]{0:T(256)} %param.11) | copy-start | bytes 3076
  5.0 29.8 %all-to-all-start = ((bf16[16,16,3200]{2,1,0:T(8,128)(2,1)}), bf16[16,16,3200]{2,1,0:T(8,128)(2,1)S(1)}, u32[]{:S(2)}, u32[]{:S(2)}) async-start(bf16[16,16,3200]{2,1,0:T(8,128)(2,1)} %bitcast.34), calls=%async_computation | async-start | bytes 3276800 | tf_op jit(solution)/shard_map/all_to_all | solution.py:439
  12.6 38.9 %collective-permute-start.3 = (bf16[4096,128]{1,0:T(8,128)(2,1)}, bf16[4096,128]{1,0:T(8,128)(2,1)}, u32[]{:S(2)}, u32[]{:S(2)}) collective-permute-start(bf16[4096,128]{1,0:T(8,128)(2,1)} %bitcast.8), channel_id=1, source_target_pairs={{0,1},{1,0},{2,3},{3,2},{4,5},{5,4},{6,7},{7,6},{8,9},{9,8},{10,11... | collective-permute-start | bytes 3145736 | tf_op jit(solution)/shard_map/ppermute | solution.py:422
  12.6 38.9 %collective-permute-start.2 = (bf16[4096,128]{1,0:T(8,128)(2,1)}, bf16[4096,128]{1,0:T(8,128)(2,1)}, u32[]{:S(2)}, u32[]{:S(2)}) collective-permute-start(bf16[4096,128]{1,0:T(8,128)(2,1)} %bitcast.7), channel_id=1, source_target_pairs={{0,1},{1,0},{2,3},{3,2},{4,5},{5,4},{6,7},{7,6},{8,9},{9,8},{10,11... | collective-permute-start | bytes 3145736 | tf_op jit(solution)/shard_map/ppermute | solution.py:422
  13.1 35.3 %collective-permute-start.4 = (bf16[128,4096]{1,0:T(8,128)(2,1)}, bf16[128,4096]{1,0:T(8,128)(2,1)}, u32[]{:S(2)}, u32[]{:S(2)}) collective-permute-start(bf16[128,4096]{1,0:T(8,128)(2,1)} %bitcast.9), channel_id=1, source_target_pairs={{0,1},{1,0},{2,3},{3,2},{4,5},{5,4},{6,7},{7,6},{8,9},{9,8},{10,11... | collective-permute-start | bytes 3145736 | tf_op jit(solution)/shard_map/ppermute | solution.py:422
  34.8 32.8 %all-to-all-start.1 = ((bf16[16,16,3968]{2,1,0:T(8,128)(2,1)}), bf16[16,16,3968]{2,1,0:T(8,128)(2,1)}, u32[]{:S(2)}, u32[]{:S(2)}) async-start(bf16[16,16,3968]{2,1,0:T(8,128)(2,1)} %bitcast.33), calls=%async_computation.1 | async-start | bytes 4063232 | tf_op jit(solution)/shard_map/all_to_all | solution.py:469
  42.4 22.5 %collective-permute-start = (bf16[128,3200]{1,0:T(8,128)(2,1)S(1)}, bf16[128,3200]{1,0:T(8,128)(2,1)S(1)}, u32[]{:S(2)}, u32[]{:S(2)}) collective-permute-start(bf16[128,3200]{1,0:T(8,128)(2,1)S(1)} %get-tuple-element.57), channel_id=1, source_target_pairs={{0,2},{2,4},{4,6},{6,8},{8,10},{10,12},{12,14},{14,0},{1,3},{3,5},... | collective-permute-start | bytes 2457608 | tf_op jit(solution)/shard_map/ppermute | solution.py:467
  44.4 20.5 %collective-permute-start.1 = (bf16[128,3200]{1,0:T(8,128)(2,1)S(1)}, bf16[128,3200]{1,0:T(8,128)(2,1)}, u32[]{:S(2)}, u32[]{:S(2)}) collective-permute-start(bf16[128,3200]{1,0:T(8,128)(2,1)S(1)} %get-tuple-element.56), channel_id=1, source_target_pairs={{0,14},{2,0},{4,2},{6,4},{8,6},{10,8},{12,10},{14,12},{1,15},{3,1}... | collective-permute-start | bytes 2457608 | tf_op jit(solution)/shard_map/ppermute | solution.py:468
  77.0 22.1 %collective-permute-start.6 = (bf16[320,1152]{1,0:T(8,128)(2,1)}, bf16[320,1152]{1,0:T(8,128)(2,1)S(1)}, u32[]{:S(2)}, u32[]{:S(2)}) collective-permute-start(bf16[320,1152]{1,0:T(8,128)(2,1)} %get-tuple-element.44), channel_id=1, source_target_pairs={{0,14},{2,0},{4,2},{6,4},{8,6},{10,8},{12,10},{14,12},{1,15},{3,1}... | collective-permute-start | bytes 2211848 | tf_op jit(solution)/shard_map/ppermute | solution.py:492
  82.9 16.2 %collective-permute-start.5 = (bf16[320,1024]{1,0:T(8,128)(2,1)}, bf16[320,1024]{1,0:T(8,128)(2,1)S(1)}, u32[]{:S(2)}, u32[]{:S(2)}) collective-permute-start(bf16[320,1024]{1,0:T(8,128)(2,1)} %get-tuple-element.43), channel_id=1, source_target_pairs={{0,2},{2,4},{4,6},{6,8},{8,10},{10,12},{12,14},{14,0},{1,3},{3,5},... | collective-permute-start | bytes 1966088 | tf_op jit(solution)/shard_map/ppermute | solution.py:491
  94.8 19.3 %collective-permute-start.10 = (bf16[4096,128]{1,0:T(8,128)(2,1)}, bf16[4096,128]{1,0:T(8,128)(2,1)S(1)}, u32[]{:S(2)}, u32[]{:S(2)}) collective-permute-start(bf16[4096,128]{1,0:T(8,128)(2,1)} %convolution_convert_fusion.2), channel_id=1, source_target_pairs={{0,1},{1,0},{2,3},{3,2},{4,5},{5,4},{6,7},{7,6},{8,9},{9,8},{10,11... | collective-permute-start | bytes 3145736 | tf_op jit(solution)/shard_map/ppermute | solution.py:500
  96.9 19.3 %collective-permute-start.11 = (bf16[4096,128]{1,0:T(8,128)(2,1)}, bf16[4096,128]{1,0:T(8,128)(2,1)}, u32[]{:S(2)}, u32[]{:S(2)}) collective-permute-start(bf16[4096,128]{1,0:T(8,128)(2,1)} %convolution_convert_fusion.1), channel_id=1, source_target_pairs={{0,1},{1,0},{2,3},{3,2},{4,5},{5,4},{6,7},{7,6},{8,9},{9,8},{10,11... | collective-permute-start | bytes 3145736 | tf_op jit(solution)/shard_map/ppermute | solution.py:500
  102.0 8.3 %copy-start.20 = (bf16[320,256]{1,0:T(8,128)(2,1)S(1)}, bf16[320,256]{1,0:T(8,128)(2,1)}, u32[]{:S(2)}) copy-start(bf16[320,256]{1,0:T(8,128)(2,1)} %get-tuple-element.53) | copy-start | bytes 491524
  102.0 28.4 %all-to-all-start.2 = ((bf16[32,16,1408]{2,1,0:T(8,128)(2,1)}), bf16[32,16,1408]{2,1,0:T(8,128)(2,1)S(1)}, u32[]{:S(2)}, u32[]{:S(2)}) async-start(bf16[32,16,1408]{2,1,0:T(8,128)(2,1)} %shard_map.130), calls=%async_computation.2 | async-start | bytes 2883584 | tf_op jit(solution)/shard_map/all_to_all | solution.py:503
  114.0 24.1 %collective-permute-start.12 = (bf16[128,4096]{1,0:T(8,128)(2,1)}, bf16[128,4096]{1,0:T(8,128)(2,1)}, u32[]{:S(2)}, u32[]{:S(2)}) collective-permute-start(bf16[128,4096]{1,0:T(8,128)(2,1)} %convolution_convert_fusion), channel_id=1, source_target_pairs={{0,1},{1,0},{2,3},{3,2},{4,5},{5,4},{6,7},{7,6},{8,9},{9,8},{10,11... | collective-permute-start | bytes 3145736 | tf_op jit(solution)/shard_map/ppermute | solution.py:500
  116.2 14.2 %copy-start.9 = (bf16[4,256,512]{2,1,0:T(8,128)(2,1)S(1)}, bf16[4,256,512]{2,1,0:T(8,128)(2,1)}, u32[]{:S(2)}) copy-start(bf16[4,256,512]{2,1,0:T(8,128)(2,1)} %copy-done.8) | copy-start | bytes 3145732
  131.8 13.8 %collective-permute-start.7 = (bf16[272,256]{1,0:T(8,128)(2,1)S(1)}, bf16[272,256]{1,0:T(8,128)(2,1)S(1)}, u32[]{:S(2)}, u32[]{:S(2)}) collective-permute-start(bf16[272,256]{1,0:T(8,128)(2,1)S(1)} %get-tuple-element.46), channel_id=1, source_target_pairs={{0,8},{2,10},{4,12},{6,14},{8,0},{10,2},{12,4},{14,6},{1,9},{3,11}... | collective-permute-start | bytes 417800 | tf_op jit(solution)/shard_map/ppermute | solution.py:512
  134.0 11.6 %collective-permute-start.8 = (bf16[272,256]{1,0:T(8,128)(2,1)S(1)}, bf16[272,256]{1,0:T(8,128)(2,1)S(1)}, u32[]{:S(2)}, u32[]{:S(2)}) collective-permute-start(bf16[272,256]{1,0:T(8,128)(2,1)S(1)} %get-tuple-element.47), channel_id=1, source_target_pairs={{0,4},{2,6},{4,8},{6,10},{8,12},{10,14},{12,0},{14,2},{1,5},{3,7},... | collective-permute-start | bytes 417800 | tf_op jit(solution)/shard_map/ppermute | solution.py:512
  135.5 13.4 %collective-permute-start.9 = (bf16[272,256]{1,0:T(8,128)(2,1)S(1)}, bf16[272,256]{1,0:T(8,128)(2,1)S(1)}, u32[]{:S(2)}, u32[]{:S(2)}) collective-permute-start(bf16[272,256]{1,0:T(8,128)(2,1)S(1)} %get-tuple-element.48), channel_id=1, source_target_pairs={{0,12},{2,14},{4,0},{6,2},{8,4},{10,6},{12,8},{14,10},{1,13},{3,15... | collective-permute-start | bytes 417800 | tf_op jit(solution)/shard_map/ppermute | solution.py:512
  (13 other events, 47.2 us)

commit v2 on v1

--- a/solution.py
+++ b/solution.py
@@ -359,16 +359,16 @@
         score = m[0:1, :] + m[1:2, :] + t[2:3, :] + t[3:4, :]
         hi = score.astype(BF).astype(F32)
         rows += [hi, score - hi]
-    row16 = iota((16, 256), 0)
-    scores = jnp.zeros((16, 256), F32)
+    row8 = iota((8, 256), 0)
+    scores = jnp.zeros((8, 256), F32)
     for n in range(4):
-        scores = jnp.where(row16 == n, rows[n], scores)
+        scores = jnp.where(row8 == n, rows[n], scores)
     scores = scores.astype(BF)
     for n in range(4):
         dest = lax.rem(z_index() + 2 * n, 8)
         at = pl.multiple_of((dest >> 1) * 256, 256)
         outs[n][0:256, :] = acc_ref[:, pl.ds(at, 256)]
-        outs[n][256:272, :] = scores
+        outs[n][256:264, :] = scores
 
 
 def final_kernel(gg_ref, ig_ref, p0, p1, p2, p3, tok_ref, group_ref, inner_ref):
@@ -424,7 +424,7 @@
     whole = lambda i: (0, 0)
     block = lambda i: (0, i)
     later = lambda i: (0, A_UNITS + i)
-    small = pltpu.CompilerParams(vmem_limit_bytes=12 * 2**20)
+    small = pltpu.CompilerParams(vmem_limit_bytes=62 * 2**20)
     a_send, ranks, ohm, oht = call(
         pack_a,
         (sds((256, A_UNITS * WIRE)), sds((8, 256), F32), sds((256, 256)), sds((64, 256))),
@@ -507,7 +507,7 @@
     upper_grad = (tdot(xs, ins[:, 256:384]) + u_par).astype(BF)
 
     pieces = call(
-        combine_kernel, (sds((272, 256)),) * 4, (WHOLE,) * 2, 8, scratch_shapes=[pltpu.VMEM((256, 1024), BF)]
+        combine_kernel, (sds((264, 256)),) * 4, (WHOLE,) * 2, 8, scratch_shapes=[pltpu.VMEM((256, 1024), BF)]
     )(masks, r1)
     got = [lax.ppermute(pieces[n], "z", around(2 * n)) for n in (2, 1, 3)]
     token_grad, group_grad, inner_grad = call(

time: 151 us -> 151 us (level)
  local copies, waits for them, and re-layouts: 7.05 us -> 2.88 us
  Pallas kernels: 26.9 us -> 29.5 us
  other arithmetic: 8.39 us -> 9.93 us
    unnamed x42 -> x28, local copies, waits for them, and re-layouts: 6.79 us -> 2.62 us
    pallas_call x1, Pallas kernels: 3.03 us -> 5.68 us  [per_device(): pl.pallas_call(pack_b, grid=(B_UNITS,), in_specs=[pl.BlockSpec((2, 256),...]
    concatenate x1, other arithmetic: 1.53 us -> 3.06 us  [per_device(): b_send = jnp.concatenate([bx, bg, wt], axis=1)]
  transfers between devices with their start and end apart: 16 -> 16, of which waited for: 7 -> 7; matrix products, arithmetic and copies ran while one was open for 18% -> 20% of each run, Pallas kernels for 8% -> 10%
where the time goes in v2:
time: 151 us; the launch traced here: 149 us
  waiting for transfers between devices  44.5 us (29%)
  starting transfers between devices  42.5 us (28%)
  Pallas kernels  29.5 us (20%)
  matrix products  19 us (13%)
  other arithmetic  9.93 us (7%)
  local copies, waits for them, and re-layouts  2.88 us (2%)
    dot_general x6, matrix products, tdot(): lax.dot_general(a, b, (((0,), (0,)), ((), ())), preferred_element_type=F32)  19 us
    all_to_all x1, waiting for transfers between devices, per_device(): lax.all_to_all(a_send.reshape(16, 16, -1), 'ep', 0, 0, tiled=True)  12.9 us
    all_to_all x1, waiting for transfers between devices, per_device(): r1 = lax.all_to_all(p1, ('ep', 'core'), 0, 0, tiled=True).reshape(512, -1)  10.9 us
    ppermute x1, waiting for transfers between devices, per_device(): z1 = lax.ppermute(a_recv[:128], 'z', around(1))  9.59 us
    pallas_call x1, Pallas kernels, per_device(): call(expert_kernel, outs, (FAR,) * 6, 63, out_specs=(FAR,) * 6, scratch_s...  9.34 us
    all_to_all x1, starting transfers between devices, per_device(): r1 = lax.all_to_all(p1, ('ep', 'core'), 0, 0, tiled=True).reshape(512, -1)  8.11 us
    all_to_all x1, starting transfers between devices, per_device(): lax.all_to_all(a_send.reshape(16, 16, -1), 'ep', 0, 0, tiled=True)  7.49 us
    all_to_all x1, starting transfers between devices, per_device(): lax.all_to_all(b_send.reshape(16, 16, -1), 'ep', 0, 0, tiled=True)  7.41 us
  transfers between devices with their start and end apart: 16, of which 7 were waited for; matrix products, arithmetic and copies ran while one was open for 20% of the time, Pallas kernels for 10%

profile of v2, /device:TPU:2, one launch (start us, length us, event | category | flops | bytes accessed | tf_op | source)
XLA Modules:
  0.0 149.1 jit_solution(14543359925706794823)
XLA Ops:
  0.6 4.3 %shard_map.127 = (bf16[256,3200]{1,0:T(8,128)(2,1)}, f32[8,256]{1,0:T(8,128)}, bf16[256,256]{1,0:T(8,128)(2,1)}, bf16[64,256]{1,0:T(8,128)(2,1)}) custom-call(s32[2,256]{1,0:T(2,128)} %bitcast.33, bf16[256,4096]{1,0:T(8,128)(2,1)} %x_ref.3, bf16[256,4096]{1,0:T(8,128)(2,1)} %g_ref.3), custom_call_target="tpu_custom_call" | custom-call | tf_op jit(solution)/shard_map/pallas_call | solution.py:428
  4.9 7.5 %all-to-all-start = ((bf16[16,16,3200]{2,1,0:T(8,128)(2,1)}), bf16[16,16,3200]{2,1,0:T(8,128)(2,1)S(1)}, u32[]{:S(2)}, u32[]{:S(2)}) async-start(bf16[16,16,3200]{2,1,0:T(8,128)(2,1)} %bitcast.32), calls=%async_computation | async-start | bytes 3276800 | tf_op jit(solution)/shard_map/all_to_all | solution.py:439
  13.0 5.7 %shard_map.128 = (bf16[256,1920]{1,0:T(8,128)(2,1)}, bf16[256,1920]{1,0:T(8,128)(2,1)}, bf16[256,128]{1,0:T(8,128)(2,1)}, bf16[4,256,512]{2,1,0:T(8,128)(2,1)}) custom-call(s32[2,256]{1,0:T(2,128)} %bitcast.34, f32[1,256]{1,0:T(1,128)} %bitcast.29, f32[2,256]{1,0:T(2,128)} %bitcast.27, f32[8,256]{1,0:T(8,128)} %get-tuple-element.31.info_ref, ...), custom_call_target="tpu_custom_call" | custom-call | tf_op jit(solution)/shard_map/pallas_call | solution.py:441
  18.7 3.1 %pad_maximum_fusion.2 = bf16[256,3968]{1,0:T(8,128)(2,1)} fusion(bf16[256,128]{1,0:T(8,128)(2,1)} %get-tuple-element.37, bf16[256,1920]{1,0:T(8,128)(2,1)} %get-tuple-element.36, bf16[256,1920]{1,0:T(8,128)(2,1)} %get-tuple-element.35), kind=kLoop, calls=%fused_computation.15 | loop fusion | flops 6094848 | bytes 4063232 | tf_op jit(solution)/shard_map/concatenate | solution.py:465
  21.8 12.9 %all-to-all-done = bf16[16,16,3200]{2,1,0:T(8,128)(2,1)S(1)} async-done(((bf16[16,16,3200]{2,1,0:T(8,128)(2,1)}), bf16[16,16,3200]{2,1,0:T(8,128)(2,1)S(1)}, u32[]{:S(2)}, u32[]{:S(2)}) %all-to-all-start) | async-done | bytes 1638432 | tf_op jit(solution)/shard_map/all_to_all | solution.py:439
  34.6 7.4 %all-to-all-start.1 = ((bf16[16,16,3968]{2,1,0:T(8,128)(2,1)}), bf16[16,16,3968]{2,1,0:T(8,128)(2,1)}, u32[]{:S(2)}, u32[]{:S(2)}) async-start(bf16[16,16,3968]{2,1,0:T(8,128)(2,1)} %bitcast.31), calls=%async_computation.1 | async-start | bytes 4063232 | tf_op jit(solution)/shard_map/all_to_all | solution.py:469
  44.1 4.0 %collective-permute-start.1 = (bf16[128,3200]{1,0:T(8,128)(2,1)S(1)}, bf16[128,3200]{1,0:T(8,128)(2,1)}, u32[]{:S(2)}, u32[]{:S(2)}) collective-permute-start(bf16[128,3200]{1,0:T(8,128)(2,1)S(1)} %get-tuple-element.56), channel_id=1, source_target_pairs={{0,14},{2,0},{4,2},{6,4},{8,6},{10,8},{12,10},{14,12},{1,15},{3,1}... | collective-permute-start | bytes 2457608 | tf_op jit(solution)/shard_map/ppermute | solution.py:468
  48.2 3.1 %pad_maximum_fusion.1.wd_hbm = bf16[256,4096]{1,0:T(8,128)(2,1)} fusion(bf16[128,4096]{1,0:T(8,128)(2,1)} %collective-permute-done.4, bf16[128,4096]{1,0:T(8,128)(2,1)} %bitcast.9), kind=kLoop, calls=%fused_computation.14 | loop fusion | flops 4194304 | bytes 4194304 | tf_op jit(solution)/shard_map/concatenate | solution.py:471
  51.3 3.7 %pad_maximum_fusion.wcat_ref = bf16[4096,512]{1,0:T(8,128)(2,1)} fusion(bf16[4096,128]{1,0:T(8,128)(2,1)} %collective-permute-done.3, bf16[4096,128]{1,0:T(8,128)(2,1)} %bitcast.8, bf16[4096,128]{1,0:T(8,128)(2,1)} %collective-permute-done.2, bf16[4096,128]{1,0:T(8,128)(2,1)} %bitcast.7), kind=kLoop, calls=%fused_computation.13 | loop fusion | flops 16777216 | bytes 8388608 | tf_op jit(solution)/shard_map/concatenate | solution.py:470
  55.0 9.6 %collective-permute-done.z1_ref = bf16[128,3200]{1,0:T(8,128)(2,1)S(1)} collective-permute-done((bf16[128,3200]{1,0:T(8,128)(2,1)S(1)}, bf16[128,3200]{1,0:T(8,128)(2,1)S(1)}, u32[]{:S(2)}, u32[]{:S(2)}) %collective-permute-start) | collective-permute-done | bytes 819232 | tf_op jit(solution)/shard_map/ppermute | solution.py:467
  64.6 2.8 %all-to-all-done.1 = bf16[16,16,3968]{2,1,0:T(8,128)(2,1)} async-done(((bf16[16,16,3968]{2,1,0:T(8,128)(2,1)}), bf16[16,16,3968]{2,1,0:T(8,128)(2,1)}, u32[]{:S(2)}, u32[]{:S(2)}) %all-to-all-start.1) | async-done | bytes 2031648 | tf_op jit(solution)/shard_map/all_to_all | solution.py:469
  67.4 9.3 %shard_map.129 = (f32[320,128]{1,0:T(8,128)}, bf16[320,256]{1,0:T(8,128)(2,1)}, bf16[320,512]{1,0:T(8,128)(2,1)}, bf16[256,128]{1,0:T(8,128)(2,1)}, bf16[320,102...) custom-call(bf16[256,3200]{1,0:T(8,128)(2,1)} %bitcast.24, bf16[128,3200]{1,0:T(8,128)(2,1)} %copy-done.3, ...), custom_call_target="tpu_custom_call" | custom-call | tf_op jit(solution)/shard_map/pallas_call | solution.py:477
  76.8 5.9 %collective-permute-start.6 = (bf16[320,1152]{1,0:T(8,128)(2,1)}, bf16[320,1152]{1,0:T(8,128)(2,1)S(1)}, u32[]{:S(2)}, u32[]{:S(2)}) collective-permute-start(bf16[320,1152]{1,0:T(8,128)(2,1)} %get-tuple-element.44), channel_id=1, source_target_pairs={{0,14},{2,0},{4,2},{6,4},{8,6},{10,8},{12,10},{14,12},{1,15},{3,1}... | collective-permute-start | bytes 2211848 | tf_op jit(solution)/shard_map/ppermute | solution.py:492
  85.3 5.3 %shard_map.133 = (bf16[320,4096]{1,0:T(8,128)(2,1)}, bf16[320,4096]{1,0:T(8,128)(2,1)}) custom-call(bf16[256,3200]{1,0:T(8,128)(2,1)S(1)} %bitcast.25, bf16[128,3200]{1,0:T(8,128)(2,1)S(1)} %copy-done.4, bf16[128,3200]{1,0:T(8,128)(2,1)} %collective-permute-done.1.z2_ref, bf16[256,3968]{1,0:T(8,128)(2,1)} %bitcast.6.b_ref), custom_call_target="tpu_custom_call" | custom-call | tf_op jit(solution)/shard_map/pallas_call | solution.py:494
  90.6 3.9 %convolution_convert_fusion.2 = bf16[4096,128]{1,0:T(8,128)(2,1)} fusion(bf16[320,4096]{1,0:T(8,128)(2,1)} %get-tuple-element.52, bf16[320,512]{1,0:T(8,128)(2,1)S(1)} %copy-done.5), kind=kOutput, calls=%fused_computation.9 | convolution fusion | flops 336068608 | bytes 3751936 | tf_op jit(solution)/shard_map/dot_general | solution.py:413
  98.9 2.8 %shard_map.130 = bf16[32,16,1408]{2,1,0:T(8,128)(2,1)} custom-call(bf16[320,512]{1,0:T(8,128)(2,1)S(1)} %copy-done.5, bf16[4096,512]{1,0:T(8,128)(2,1)S(1)} %copy-done, bf16[256,128]{1,0:T(8,128)(2,1)S(1)} %copy-done.7, bf16[320,1024]{1,0:T(8,128)(2,1)S(1)} %collective-permute-done.5.up_ref, bf16[320,1152]{1,0:T(8,128)(2,1)S(1)} %collective-permute-done.6.dn_ref), custom_call_target="tpu_custom_call" | custom-call | tf_op jit(solution)/shard_map/pallas_call | solution.py:502
  101.8 8.1 %all-to-all-start.2 = ((bf16[32,16,1408]{2,1,0:T(8,128)(2,1)}), bf16[32,16,1408]{2,1,0:T(8,128)(2,1)S(1)}, u32[]{:S(2)}, u32[]{:S(2)}) async-start(bf16[32,16,1408]{2,1,0:T(8,128)(2,1)} %shard_map.130), calls=%async_computation.2 | async-start | bytes 2883584 | tf_op jit(solution)/shard_map/all_to_all | solution.py:503
  110.1 3.7 %convolution_convert_fusion = bf16[128,4096]{1,0:T(8,128)(2,1)} fusion(bf16[320,4096]{1,0:T(8,128)(2,1)} %get-tuple-element.55, f32[320]{0:T(512)S(1)} %slice_reduce_fusion, bf16[320,256]{1,0:T(8,128)(2,1)S(1)} %copy-done.13), kind=kOutput, calls=%fused_computation.7 | convolution fusion | flops 340000768 | bytes 3753984 | tf_op jit(solution)/shard_map/dot_general | solution.py:413
  116.0 3.4 %fusion.4 = bf16[1,4096,128]{2,1,0:T(8,128)(2,1)} fusion(bf16[320,4096]{1,0:T(8,128)(2,1)S(1)} %copy-done.11, bf16[4096,128]{1,0:T(8,128)(2,1)} %collective-permute-done.11, bf16[320,512]{1,0:T(8,128)(2,1)S(1)} %copy-done.5), kind=kOutput, calls=%fused_computation.11 | convolution fusion | flops 337117184 | bytes 4800512 | tf_op jit(solution)/shard_map/dot_general | solution.py:413
  119.4 10.9 %all-to-all-done.2 = bf16[32,16,1408]{2,1,0:T(8,128)(2,1)S(1)} async-done(((bf16[32,16,1408]{2,1,0:T(8,128)(2,1)}), bf16[32,16,1408]{2,1,0:T(8,128)(2,1)S(1)}, u32[]{:S(2)}, u32[]{:S(2)}) %all-to-all-start.2) | async-done | bytes 1441824 | tf_op jit(solution)/shard_map/all_to_all | solution.py:503
  135.3 2.7 %collective-permute-start.9 = (bf16[264,256]{1,0:T(8,128)(2,1)S(1)}, bf16[264,256]{1,0:T(8,128)(2,1)S(1)}, u32[]{:S(2)}, u32[]{:S(2)}) collective-permute-start(bf16[264,256]{1,0:T(8,128)(2,1)S(1)} %get-tuple-element.48), channel_id=1, source_target_pairs={{0,12},{2,14},{4,0},{6,2},{8,4},{10,6},{12,8},{14,10},{1,13},{3,15... | collective-permute-start | bytes 405512 | tf_op jit(solution)/shard_map/ppermute | solution.py:512
  137.9 3.9 %fusion.3 = bf16[1,128,4096]{2,1,0:T(8,128)(2,1)} fusion(bf16[128,4096]{1,0:T(8,128)(2,1)} %collective-permute-done.12, bf16[320,4096]{1,0:T(8,128)(2,1)} %get-tuple-element.55, f32[320]{0:T(512)S(1)} %slice_reduce_fusion, bf16[320,256]{1,0:T(8,128)(2,1)S(1)} %copy-done.13), kind=kOutput, calls=%fused_computation.10 | convolution fusion | flops 341049344 | bytes 4802560 | tf_op jit(solution)/shard_map/dot_general | solution.py:413
  141.8 3.4 %collective-permute-done.7.p1 = bf16[264,256]{1,0:T(8,128)(2,1)S(1)} collective-permute-done((bf16[264,256]{1,0:T(8,128)(2,1)S(1)}, bf16[264,256]{1,0:T(8,128)(2,1)S(1)}, u32[]{:S(2)}, u32[]{:S(2)}) %collective-permute-start.7) | collective-permute-done | bytes 135200 | tf_op jit(solution)/shard_map/ppermute | solution.py:512
  145.2 3.1 %collective-permute-done.9.p3 = bf16[264,256]{1,0:T(8,128)(2,1)S(1)} collective-permute-done((bf16[264,256]{1,0:T(8,128)(2,1)S(1)}, bf16[264,256]{1,0:T(8,128)(2,1)S(1)}, u32[]{:S(2)}, u32[]{:S(2)}) %collective-permute-start.9) | collective-permute-done | bytes 135200 | tf_op jit(solution)/shard_map/ppermute | solution.py:512
  (54 shorter events, 17.8 us)
Async XLA Ops:
  4.9 29.7 %all-to-all-start = ((bf16[16,16,3200]{2,1,0:T(8,128)(2,1)}), bf16[16,16,3200]{2,1,0:T(8,128)(2,1)S(1)}, u32[]{:S(2)}, u32[]{:S(2)}) async-start(bf16[16,16,3200]{2,1,0:T(8,128)(2,1)} %bitcast.32), calls=%async_computation | async-start | bytes 3276800 | tf_op jit(solution)/shard_map/all_to_all | solution.py:439
  12.4 38.9 %collective-permute-start.3 = (bf16[4096,128]{1,0:T(8,128)(2,1)}, bf16[4096,128]{1,0:T(8,128)(2,1)}, u32[]{:S(2)}, u32[]{:S(2)}) collective-permute-start(bf16[4096,128]{1,0:T(8,128)(2,1)} %bitcast.8), channel_id=1, source_target_pairs={{0,1},{1,0},{2,3},{3,2},{4,5},{5,4},{6,7},{7,6},{8,9},{9,8},{10,11... | collective-permute-start | bytes 3145736 | tf_op jit(solution)/shard_map/ppermute | solution.py:422
  12.4 38.9 %collective-permute-start.2 = (bf16[4096,128]{1,0:T(8,128)(2,1)}, bf16[4096,128]{1,0:T(8,128)(2,1)}, u32[]{:S(2)}, u32[]{:S(2)}) collective-permute-start(bf16[4096,128]{1,0:T(8,128)(2,1)} %bitcast.7), channel_id=1, source_target_pairs={{0,1},{1,0},{2,3},{3,2},{4,5},{5,4},{6,7},{7,6},{8,9},{9,8},{10,11... | collective-permute-start | bytes 3145736 | tf_op jit(solution)/shard_map/ppermute | solution.py:422
  12.9 35.3 %collective-permute-start.4 = (bf16[128,4096]{1,0:T(8,128)(2,1)}, bf16[128,4096]{1,0:T(8,128)(2,1)}, u32[]{:S(2)}, u32[]{:S(2)}) collective-permute-start(bf16[128,4096]{1,0:T(8,128)(2,1)} %bitcast.9), channel_id=1, source_target_pairs={{0,1},{1,0},{2,3},{3,2},{4,5},{5,4},{6,7},{7,6},{8,9},{9,8},{10,11... | collective-permute-start | bytes 3145736 | tf_op jit(solution)/shard_map/ppermute | solution.py:422
  34.6 7.5 %copy-start.1 = (bf16[16,16,3200]{2,1,0:T(8,128)(2,1)}, bf16[16,16,3200]{2,1,0:T(8,128)(2,1)S(1)}, u32[]{:S(2)}) copy-start(bf16[16,16,3200]{2,1,0:T(8,128)(2,1)S(1)} %all-to-all-done) | copy-start | bytes 4915204
  34.6 32.8 %all-to-all-start.1 = ((bf16[16,16,3968]{2,1,0:T(8,128)(2,1)}), bf16[16,16,3968]{2,1,0:T(8,128)(2,1)}, u32[]{:S(2)}, u32[]{:S(2)}) async-start(bf16[16,16,3968]{2,1,0:T(8,128)(2,1)} %bitcast.31), calls=%async_computation.1 | async-start | bytes 4063232 | tf_op jit(solution)/shard_map/all_to_all | solution.py:469
  42.1 22.5 %collective-permute-start = (bf16[128,3200]{1,0:T(8,128)(2,1)S(1)}, bf16[128,3200]{1,0:T(8,128)(2,1)S(1)}, u32[]{:S(2)}, u32[]{:S(2)}) collective-permute-start(bf16[128,3200]{1,0:T(8,128)(2,1)S(1)} %get-tuple-element.57), channel_id=1, source_target_pairs={{0,2},{2,4},{4,6},{6,8},{8,10},{10,12},{12,14},{14,0},{1,3},{3,5},... | collective-permute-start | bytes 2457608 | tf_op jit(solution)/shard_map/ppermute | solution.py:467
  44.1 20.5 %collective-permute-start.1 = (bf16[128,3200]{1,0:T(8,128)(2,1)S(1)}, bf16[128,3200]{1,0:T(8,128)(2,1)}, u32[]{:S(2)}, u32[]{:S(2)}) collective-permute-start(bf16[128,3200]{1,0:T(8,128)(2,1)S(1)} %get-tuple-element.56), channel_id=1, source_target_pairs={{0,14},{2,0},{4,2},{6,4},{8,6},{10,8},{12,10},{14,12},{1,15},{3,1}... | collective-permute-start | bytes 2457608 | tf_op jit(solution)/shard_map/ppermute | solution.py:468
  76.8 22.2 %collective-permute-start.6 = (bf16[320,1152]{1,0:T(8,128)(2,1)}, bf16[320,1152]{1,0:T(8,128)(2,1)S(1)}, u32[]{:S(2)}, u32[]{:S(2)}) collective-permute-start(bf16[320,1152]{1,0:T(8,128)(2,1)} %get-tuple-element.44), channel_id=1, source_target_pairs={{0,14},{2,0},{4,2},{6,4},{8,6},{10,8},{12,10},{14,12},{1,15},{3,1}... | collective-permute-start | bytes 2211848 | tf_op jit(solution)/shard_map/ppermute | solution.py:492
  82.7 16.2 %collective-permute-start.5 = (bf16[320,1024]{1,0:T(8,128)(2,1)}, bf16[320,1024]{1,0:T(8,128)(2,1)S(1)}, u32[]{:S(2)}, u32[]{:S(2)}) collective-permute-start(bf16[320,1024]{1,0:T(8,128)(2,1)} %get-tuple-element.43), channel_id=1, source_target_pairs={{0,2},{2,4},{4,6},{6,8},{8,10},{10,12},{12,14},{14,0},{1,3},{3,5},... | collective-permute-start | bytes 1966088 | tf_op jit(solution)/shard_map/ppermute | solution.py:491
  85.3 5.3 %copy-start.5 = (bf16[320,512]{1,0:T(8,128)(2,1)S(1)}, bf16[320,512]{1,0:T(8,128)(2,1)}, u32[]{:S(2)}) copy-start(bf16[320,512]{1,0:T(8,128)(2,1)} %get-tuple-element.41.in_ref) | copy-start | bytes 983044
  94.5 4.4 %copy-start.7 = (bf16[256,128]{1,0:T(8,128)(2,1)S(1)}, bf16[256,128]{1,0:T(8,128)(2,1)}, u32[]{:S(2)}) copy-start(bf16[256,128]{1,0:T(8,128)(2,1)} %get-tuple-element.42.sc_ref) | copy-start | bytes 196612
  94.5 19.4 %collective-permute-start.10 = (bf16[4096,128]{1,0:T(8,128)(2,1)}, bf16[4096,128]{1,0:T(8,128)(2,1)S(1)}, u32[]{:S(2)}, u32[]{:S(2)}) collective-permute-start(bf16[4096,128]{1,0:T(8,128)(2,1)} %convolution_convert_fusion.2), channel_id=1, source_target_pairs={{0,1},{1,0},{2,3},{3,2},{4,5},{5,4},{6,7},{7,6},{8,9},{9,8},{10,11... | collective-permute-start | bytes 3145736 | tf_op jit(solution)/shard_map/ppermute | solution.py:500
  96.6 19.4 %collective-permute-start.11 = (bf16[4096,128]{1,0:T(8,128)(2,1)}, bf16[4096,128]{1,0:T(8,128)(2,1)}, u32[]{:S(2)}, u32[]{:S(2)}) collective-permute-start(bf16[4096,128]{1,0:T(8,128)(2,1)} %convolution_convert_fusion.1), channel_id=1, source_target_pairs={{0,1},{1,0},{2,3},{3,2},{4,5},{5,4},{6,7},{7,6},{8,9},{9,8},{10,11... | collective-permute-start | bytes 3145736 | tf_op jit(solution)/shard_map/ppermute | solution.py:500
  101.8 8.1 %copy-start.12 = (f32[320,128]{1,0:T(8,128)S(1)}, f32[320,128]{1,0:T(8,128)}, u32[]{:S(2)}) copy-start(f32[320,128]{1,0:T(8,128)} %get-tuple-element.54) | copy-start | bytes 491524
  101.8 8.3 %copy-start.13 = (bf16[320,256]{1,0:T(8,128)(2,1)S(1)}, bf16[320,256]{1,0:T(8,128)(2,1)}, u32[]{:S(2)}) copy-start(bf16[320,256]{1,0:T(8,128)(2,1)} %get-tuple-element.53) | copy-start | bytes 491524
  101.8 28.4 %all-to-all-start.2 = ((bf16[32,16,1408]{2,1,0:T(8,128)(2,1)}), bf16[32,16,1408]{2,1,0:T(8,128)(2,1)S(1)}, u32[]{:S(2)}, u32[]{:S(2)}) async-start(bf16[32,16,1408]{2,1,0:T(8,128)(2,1)} %shard_map.130), calls=%async_computation.2 | async-start | bytes 2883584 | tf_op jit(solution)/shard_map/all_to_all | solution.py:503
  113.8 24.1 %collective-permute-start.12 = (bf16[128,4096]{1,0:T(8,128)(2,1)}, bf16[128,4096]{1,0:T(8,128)(2,1)}, u32[]{:S(2)}, u32[]{:S(2)}) collective-permute-start(bf16[128,4096]{1,0:T(8,128)(2,1)} %convolution_convert_fusion), channel_id=1, source_target_pairs={{0,1},{1,0},{2,3},{3,2},{4,5},{5,4},{6,7},{7,6},{8,9},{9,8},{10,11... | collective-permute-start | bytes 3145736 | tf_op jit(solution)/shard_map/ppermute | solution.py:500
  116.0 14.2 %copy-start.6 = (bf16[4,256,512]{2,1,0:T(8,128)(2,1)S(1)}, bf16[4,256,512]{2,1,0:T(8,128)(2,1)}, u32[]{:S(2)}) copy-start(bf16[4,256,512]{2,1,0:T(8,128)(2,1)} %get-tuple-element.34.mask_ref) | copy-start | bytes 3145732
  131.6 16.8 %copy-start.8 = (f32[256,2]{0,1:T(2,128)S(1)}, f32[256,2]{0,1:T(2,128)}, u32[]{:S(2)}) copy-start(f32[256,2]{0,1:T(2,128)} %param.12) | copy-start | bytes 6148
  131.6 16.8 %copy-start.9 = (f32[256]{0:T(256)S(1)}, f32[256]{0:T(256)}, u32[]{:S(2)}) copy-start(f32[256]{0:T(256)} %param.11) | copy-start | bytes 3076
  131.6 13.6 %collective-permute-start.7 = (bf16[264,256]{1,0:T(8,128)(2,1)S(1)}, bf16[264,256]{1,0:T(8,128)(2,1)S(1)}, u32[]{:S(2)}, u32[]{:S(2)}) collective-permute-start(bf16[264,256]{1,0:T(8,128)(2,1)S(1)} %get-tuple-element.46), channel_id=1, source_target_pairs={{0,8},{2,10},{4,12},{6,14},{8,0},{10,2},{12,4},{14,6},{1,9},{3,11}... | collective-permute-start | bytes 405512 | tf_op jit(solution)/shard_map/ppermute | solution.py:512
  133.8 11.4 %collective-permute-start.8 = (bf16[264,256]{1,0:T(8,128)(2,1)S(1)}, bf16[264,256]{1,0:T(8,128)(2,1)S(1)}, u32[]{:S(2)}, u32[]{:S(2)}) collective-permute-start(bf16[264,256]{1,0:T(8,128)(2,1)S(1)} %get-tuple-element.47), channel_id=1, source_target_pairs={{0,4},{2,6},{4,8},{6,10},{8,12},{10,14},{12,0},{14,2},{1,5},{3,7},... | collective-permute-start | bytes 405512 | tf_op jit(solution)/shard_map/ppermute | solution.py:512
  135.3 13.1 %collective-permute-start.9 = (bf16[264,256]{1,0:T(8,128)(2,1)S(1)}, bf16[264,256]{1,0:T(8,128)(2,1)S(1)}, u32[]{:S(2)}, u32[]{:S(2)}) collective-permute-start(bf16[264,256]{1,0:T(8,128)(2,1)S(1)} %get-tuple-element.48), channel_id=1, source_target_pairs={{0,12},{2,14},{4,0},{6,2},{8,4},{10,6},{12,8},{14,10},{1,13},{3,15... | collective-permute-start | bytes 405512 | tf_op jit(solution)/shard_map/ppermute | solution.py:512
  (6 other events, 17.7 us)
